TPU v7x, 32 devices: a whole 2x2x4 slice. The times are simulated.
32 devices in a mesh: sp: 16 (over z, y, core), tp: 2 (over x).
Axes of the slice: x: 2, y: 2, z: 4, core: 2. Of those that a mesh axis runs over, the one named last changes fastest.
Arguments:
- queries: bfloat16 [3072, 1024], P('sp', 'tp'), may hold values from -6 to 6
- keys: bfloat16 [3072, 512], P('sp', 'tp'), may hold values from -6 to 6
- values: bfloat16 [3072, 512], P('sp', 'tp'), may hold values from -6 to 6
- q_gain: float32 [64], replicated, may hold values from 0.1 to 6.5
- k_gain: float32 [64], replicated, may hold values from 0.1 to 6.5
- w_out: bfloat16 [1024, 2048], P('tp'), may hold values from -12 to 12
- residual: bfloat16 [3072, 2048], P(('sp', 'tp')), may hold values from -6 to 6
- norm_gain: float32 [2048], replicated, may hold values from 0.1 to 1.9
- w_gate: bfloat16 [2048, 5632], P('sp', 'tp'), may hold values from -0.125 to 0.125
- w_up: bfloat16 [2048, 5632], P('sp', 'tp'), may hold values from -0.125 to 0.125
- w_down: bfloat16 [5632, 2048], P('tp', 'sp'), may hold values from -0.25 to 0.25
Outputs:
- layer_out: bfloat16 [3072, 2048], P(('sp', 'tp'))
All inputs are finite; a program needn't handle non-finite values.
Results may differ from a plain program's by a relative error of at most 0.018.
The roundings to bfloat16 on the way count: a program that leaves them out, or rounds other values in their place, can miss the bound.
Values may be sent and summed in bfloat16 or wider, within the bound.
A program may use at most 128 MiB of HBM per device.

v0:
```python
import functools
import math

import jax
import jax.numpy as jnp
from jax import lax
from jax.experimental import pallas as pl
from jax.experimental.pallas import tpu as pltpu
from jax.sharding import PartitionSpec as P

GRID_W = 128


EPS = 1e-06
THETA = 10000.0


def turn_half(part, angle):
    quarter = part.shape[-1] // 2
    cos_table = jnp.cos(angle)[:, None, :]
    sin_table = jnp.sin(angle)[:, None, :]
    first_part = part[..., :quarter]
    second_part = part[..., quarter:]
    return jnp.concatenate(
        [
            first_part * cos_table - second_part * sin_table,
            first_part * sin_table + second_part * cos_table,
        ],
        axis=-1,
    )


def head_norm_rope(flat, gain, offset, head_count):
    tok_rows = flat.shape[0]
    head_size = flat.shape[1] // head_count
    heads = flat.astype(jnp.float32).reshape(tok_rows, head_count, head_size)
    heads = heads * lax.rsqrt(jnp.mean(heads * heads, axis=-1, keepdims=True) + EPS) * gain
    positions = offset + jnp.arange(tok_rows, dtype=jnp.int32)
    row_pos = (positions // GRID_W).astype(jnp.float32)
    col_pos = (positions % GRID_W).astype(jnp.float32)
    half_size = head_size // 2
    inv_freq = THETA ** (-jnp.arange(0, half_size, 2, dtype=jnp.float32) / half_size)
    turned = jnp.concatenate(
        [
            turn_half(heads[..., :half_size], row_pos[:, None] * inv_freq[None, :]),
            turn_half(heads[..., half_size:], col_pos[:, None] * inv_freq[None, :]),
        ],
        axis=-1,
    )
    return turned.reshape(tok_rows, head_count * head_size).astype(jnp.bfloat16)


def body(queries, keys, values, q_gain, k_gain, w_out, residual, norm_gain, w_gate, w_up, w_down):
    tok_rows = queries.shape[0]
    head_size = q_gain.shape[0]
    q_heads = queries.shape[1] // head_size
    kv_heads = keys.shape[1] // head_size
    q_group = q_heads // kv_heads
    offset = lax.axis_index("sp") * tok_rows
    q_rot = head_norm_rope(queries, q_gain, offset, q_heads)
    k_rot = head_norm_rope(keys, k_gain, offset, kv_heads)
    query_groups = q_rot.reshape(tok_rows, kv_heads, q_group, head_size)
    score_scale = head_size ** (-0.5)
    start_state = (
        jnp.full((kv_heads, q_group, tok_rows), -1e30, jnp.float32),
        jnp.zeros((kv_heads, q_group, tok_rows), jnp.float32),
        jnp.zeros((kv_heads, q_group, tok_rows, head_size), jnp.float32),
    )
    running = start_state
    key_piece = lax.all_gather(k_rot, "sp", axis=0, tiled=True)
    value_piece = lax.all_gather(values, "sp", axis=0, tiled=True)
    piece_len = key_piece.shape[0]
    block_len = math.gcd(piece_len, 512)
    blocks = piece_len // block_len
    key_blocks = key_piece.reshape(blocks, block_len, kv_heads, head_size)
    value_blocks = value_piece.reshape(blocks, block_len, kv_heads, head_size)

    def update(state, block_pair):
        prior_max, totals, accum = state
        key_block, value_block = block_pair
        scores = (
            jnp.einsum(
                "qhgd,khd->hgqk", query_groups, key_block, preferred_element_type=jnp.float32
            )
            * score_scale
        )
        new_max = jnp.maximum(prior_max, jnp.max(scores, axis=-1))
        weights = jnp.exp(scores - new_max[..., None])
        factor = jnp.exp(prior_max - new_max)
        totals = totals * factor + jnp.sum(weights, axis=-1)
        accum = accum * factor[..., None] + jnp.einsum(
            "hgqk,khd->hgqd",
            weights.astype(jnp.bfloat16),
            value_block,
            preferred_element_type=jnp.float32,
        )
        return ((new_max, totals, accum), None)

    running, unused = lax.scan(update, running, (key_blocks, value_blocks))
    final_max, totals, accum = running
    mixed = accum / totals[..., None]
    attn = (
        jnp.transpose(mixed, (2, 0, 1, 3))
        .reshape(tok_rows, q_heads * head_size)
        .astype(jnp.bfloat16)
    )
    own_rows = lax.all_to_all(attn, "tp", split_axis=0, concat_axis=1, tiled=True)
    columns = own_rows
    proj = jnp.dot(
        columns, lax.all_gather(w_out, "tp", axis=0, tiled=True), preferred_element_type=jnp.float32
    )
    mid = residual.astype(jnp.float32) + proj
    normed = (
        mid * lax.rsqrt(jnp.mean(mid * mid, axis=-1, keepdims=True) + EPS) * norm_gain
    ).astype(jnp.bfloat16)
    gathered = lax.all_gather(normed, "tp", axis=0, tiled=True)
    columns = gathered
    gate = jnp.dot(
        columns,
        lax.all_gather(w_gate, "sp", axis=0, tiled=True),
        preferred_element_type=jnp.float32,
    )
    up_part = jnp.dot(
        columns, lax.all_gather(w_up, "sp", axis=0, tiled=True), preferred_element_type=jnp.float32
    )
    hidden = (jax.nn.silu(gate) * up_part).astype(jnp.bfloat16)
    terms = jnp.dot(
        hidden, lax.all_gather(w_down, "sp", axis=1, tiled=True), preferred_element_type=jnp.float32
    )
    down = lax.psum_scatter(
        terms.astype(jnp.bfloat16), "tp", scatter_dimension=0, tiled=True
    ).astype(jnp.float32)
    return (mid + 0.5 * down).astype(jnp.bfloat16)


MESH = pl.DeviceIdType.MESH


def physical_ring(mesh):
    count = mesh.shape["sp"]
    try:
        places = [(tuple(d.coords), d.core_on_chip) for d in mesh.devices[:, 0].flat]
    except AttributeError:
        return None
    if count % 4 or count < 12 or mesh.shape["tp"] != 2:
        return None
    first = places[0][0]
    depth = count // 4
    for at, (coords, core) in enumerate(places):
        chip = at // 2
        want = (first[0], first[1] + chip % 2, first[2] + chip // 2)
        if coords != want or core != at % 2:
            return None
    return depth


def turned_heads(head_size, x_ref, g_ref, cos_ref, sin_ref):
    x = x_ref[...].astype(jnp.float32)
    width = x.shape[1]
    lane = lax.broadcasted_iota(jnp.int32, (width, width), 0) // head_size
    other = lax.broadcasted_iota(jnp.int32, (width, width), 1) // head_size
    same = (lane == other).astype(jnp.float32)
    mean = jnp.dot(
        x * x, same, preferred_element_type=jnp.float32, precision=lax.Precision.HIGHEST
    ) * (1.0 / head_size)
    h = x * lax.rsqrt(mean + EPS) * jnp.concatenate([g_ref[...]] * (width // head_size), axis=1)
    quarter = head_size // 4
    repeats = width // cos_ref.shape[1]
    cos_table = jnp.concatenate([cos_ref[...]] * repeats, axis=1)
    sin_table = jnp.concatenate([sin_ref[...]] * repeats, axis=1)
    at = lax.broadcasted_iota(jnp.int32, x.shape, 1)
    is_first = (at // quarter) % 2 == 0
    ahead = pltpu.roll(h, width - quarter, 1)
    behind = pltpu.roll(h, quarter, 1)
    turned = h * cos_table + jnp.where(is_first, -ahead, behind) * sin_table
    return turned.astype(jnp.bfloat16)


def layer_kernel(
    depth, head_size,
    raw_q, raw_k, raw_v, qg_ref, kg_ref, cos_ref, sin_ref, res_ref, gain_ref, wo_in, wg_in, wu_in, wd_in,
    out_ref,
    q_ref, kv_in, kv_all, wg_all, wu_all, wd_all, wo_own, wo_other, attn, context, context_in, mid, normed, hidden,
    terms, kept, leaving, coming,
    own_sem, ring_send, ring_recv, sib_send, sib_recv, x_send, x_recv,
):
    n = 2 * depth
    sp = lax.axis_index("sp")
    tp = lax.axis_index("tp")
    core = sp % 2
    z = sp // 4
    y = (sp // 2) % 2
    pos = (1 - y) * z + y * (n - 1 - z)

    def at_pos(p, c):
        p = lax.rem(p + n, n)
        yy = p // depth
        zz = (1 - yy) * p + yy * (n - 1 - p)
        return (zz * 2 + yy) * 2 + c

    sibling = (at_pos(pos, 1 - core), tp)
    partner = (sp, 1 - tp)
    toward = ((at_pos(pos + 1, core), tp), (at_pos(pos - 1, core), tp))

    barrier = pltpu.get_barrier_semaphore()
    for target in (sibling, partner) + toward:
        pl.semaphore_signal(barrier, inc=1, device_id=target, device_id_type=MESH)
    pl.semaphore_wait(barrier, 4)

    tok = kv_in.shape[0]
    rows = wg_in.shape[0]
    units, lanes_down = wd_in.shape
    KV, GATE, UP, LOW, HIGH = range(5)

    def half(size, way, base=0):
        return pl.ds(base + way * (size // 2), size // 2)

    def part(start, size, way):
        return pl.ds(pl.multiple_of(start * size + way * (size // 2), size // 2), size // 2)

    def columns(o):
        return pl.ds(pl.multiple_of(o * lanes_down, lanes_down), lanes_down)

    ins = (
        lambda way: kv_in.at[half(tok, way), :],
        lambda way: wg_in.at[half(rows, way), :],
        lambda way: wu_in.at[half(rows, way), :],
        lambda way: wd_in.at[half(units // 2, way), :],
        lambda way: wd_in.at[half(units // 2, way, units // 2), :],
    )
    outs = (
        lambda o, way: kv_all.at[part(o, tok, way), :],
        lambda o, way: wg_all.at[part(o, rows, way), :],
        lambda o, way: wu_all.at[part(o, rows, way), :],
        lambda o, way: wd_all.at[half(units // 2, way), columns(o)],
        lambda o, way: wd_all.at[half(units // 2, way, units // 2), columns(o)],
    )
    own_outs = (
        kv_all.at[pl.ds(pl.multiple_of(sp * tok, tok), tok), :],
        wg_all.at[pl.ds(pl.multiple_of(sp * rows, rows), rows), :],
        wu_all.at[pl.ds(pl.multiple_of(sp * rows, rows), rows), :],
        wd_all.at[:, columns(sp)],
        wo_own,
    )
    own = [
        pltpu.make_async_copy(src, dst, own_sem.at[i])
        for i, (src, dst) in enumerate(zip((kv_in, wg_in, wu_in, wd_in, wo_in), own_outs))
    ]

    def owner(step, way, c):
        return at_pos(pos - step if way == 0 else pos + step, c)

    def remote(src, dst, send_sem, recv_sem, target):
        return pltpu.make_async_remote_copy(
            src_ref=src, dst_ref=dst, send_sem=send_sem, recv_sem=recv_sem,
            device_id=target, device_id_type=MESH,
        )

    def ring(kind, step, way):
        o = owner(step, way, core)
        src = ins[kind](way) if step == 0 else outs[kind](o, way)
        return remote(
            src, outs[kind](o, way),
            ring_send.at[kind, step, way], ring_recv.at[kind, step, way], toward[way],
        )

    def arrived(kind, step, way):
        piece = outs[kind](owner(step + 1, way, core), way)
        remote(
            piece, piece,
            ring_send.at[kind, step, way], ring_recv.at[kind, step, way], toward[way],
        ).wait_recv()

    def across(kind, step, way):
        o = owner(step, way, core)
        src = ins[kind](way) if step == 0 else outs[kind](o, way)
        return remote(
            src, outs[kind](o, way),
            sib_send.at[kind, step, way], sib_recv.at[kind, step, way], sibling,
        )

    def serve(kind, step):
        for way in range(2):
            if step > 0:
                arrived(kind, step - 1, way)
            if step < n - 1:
                ring(kind, step, way).start()
            across(kind, step, way).start()

    def sibling_gave(kind, steps):
        for step in steps:
            for way in range(2):
                piece = outs[kind](owner(step, way, 1 - core), way)
                remote(
                    piece, piece,
                    sib_send.at[kind, step, way], sib_recv.at[kind, step, way], sibling,
                ).wait_recv()

    pairs, q_rows, lanes = q_ref.shape
    block = math.gcd(q_rows, 256)
    per_pair = q_rows // block

    def attend(at):
        pair, which = at // per_pair, at % per_pair
        span = slice(which * block, (which + 1) * block)
        q = q_ref[pair, span, :]
        k = kv_all[:, pair * lanes:(pair + 1) * lanes]
        v = kv_all[:, (pairs + pair) * lanes:(pairs + pair + 1) * lanes]
        scores = lax.dot_general(
            q, k, (((1,), (1,)), ((), ())), preferred_element_type=jnp.float32
        )
        weights = jnp.exp(scores - jnp.max(scores, axis=-1, keepdims=True))
        total = jnp.sum(weights, axis=-1, keepdims=True)
        mixed = jnp.dot(weights.astype(jnp.bfloat16), v, preferred_element_type=jnp.float32)
        attn[pair, span, :] = (mixed / total).astype(jnp.bfloat16)

    width = wo_in.shape[1]

    def assemble():
        group = q_rows // (2 * tok)
        blocks = []
        for pair in range(pairs):
            for side in range(2):
                for g in range(0, group, 2):
                    lower = attn[pair, pl.ds((side * group + g) * tok, tok), :].astype(jnp.float32)
                    upper = attn[pair, pl.ds((side * group + g + 1) * tok, tok), :].astype(jnp.float32)
                    if side == 1:
                        lower = pltpu.roll(lower, head_size, 1)
                    else:
                        upper = pltpu.roll(upper, head_size, 1)
                    lane = lax.broadcasted_iota(jnp.int32, lower.shape, 1)
                    blocks.append(jnp.where(lane < head_size, lower, upper).astype(jnp.bfloat16))
        context[...] = jnp.concatenate(blocks, axis=1)

    own_count = res_ref.shape[0]
    mine = pl.ds(pl.multiple_of(tp * own_count, own_count), own_count)
    theirs = pl.ds(pl.multiple_of((1 - tp) * own_count, own_count), own_count)
    give_context = remote(context.at[theirs, :], context_in, x_send.at[0], x_recv.at[0], partner)
    give_wo = remote(wo_in, wo_other, x_send.at[2 + n], x_recv.at[2 + n], partner)
    give_normed = remote(
        normed.at[mine, :], normed.at[mine, :], x_send.at[1], x_recv.at[1], partner
    )
    take_normed = remote(
        normed.at[theirs, :], normed.at[theirs, :], x_send.at[1], x_recv.at[1], partner
    )

    def normalize():
        give_context.wait_recv()
        give_wo.wait_recv()
        own[4].wait()
        held, other = context[mine, :], context_in[...]
        wide = math.gcd(width, 512)
        for at in range(0, width, wide):
            cols = slice(at, at + wide)
            mid[:, cols] = res_ref[:, cols].astype(jnp.float32) + (
                jnp.dot(held, wo_own[:, cols], preferred_element_type=jnp.float32)
                + jnp.dot(other, wo_other[:, cols], preferred_element_type=jnp.float32)
            )
        value = mid[...]
        scale = lax.rsqrt(jnp.mean(value * value, axis=-1, keepdims=True) + EPS)
        normed[mine, :] = (value * scale * gain_ref[...]).astype(jnp.bfloat16)

    tile = math.gcd(units, 256)

    def feed(first, last):
        @pl.loop(first, last)
        def _(at):
            cols = pl.ds(pl.multiple_of(at * tile, tile), tile)
            x = normed[...]
            gate = jnp.dot(x, wg_all[:, cols], preferred_element_type=jnp.float32)
            up = jnp.dot(x, wu_all[:, cols], preferred_element_type=jnp.float32)
            hidden[:, cols] = (gate / (1.0 + jnp.exp(-gate)) * up).astype(jnp.bfloat16)

    def pair_columns(d):
        o = at_pos(pos - d, 0)
        return pl.ds(pl.multiple_of(o * lanes_down, 2 * lanes_down), 2 * lanes_down)

    def give_terms(d):
        return remote(leaving.at[d], coming.at[d], x_send.at[2 + d], x_recv.at[2 + d], partner)

    def lower(d):
        terms[...] = jnp.dot(
            hidden[...], wd_all[:, pair_columns(d)], preferred_element_type=jnp.float32
        )
        kept[d] = terms[mine, :]
        leaving[d] = terms[theirs, :].astype(jnp.bfloat16)

    def emit(d):
        give_terms(d).wait_recv()
        cols = pair_columns(d)
        down = kept[d] + coming[d].astype(jnp.float32)
        out_ref[:, cols] = (mid[:, cols] + 0.5 * down).astype(jnp.bfloat16)

    for copy in own[1:]:
        copy.start()
    serve(GATE, 0)
    k_width = raw_k.shape[1]
    kv_in[:, :k_width] = turned_heads(head_size, raw_k, kg_ref, cos_ref, sin_ref)
    kv_in[:, k_width:] = raw_v[...]
    turned = turned_heads(head_size, raw_q, qg_ref, cos_ref, sin_ref).astype(jnp.float32)
    turned = turned * head_size ** (-0.5)
    group = q_rows // (2 * tok)
    for at in range(raw_q.shape[1] // lanes):
        both = turned[:, at * lanes:(at + 1) * lanes]
        swapped = pltpu.roll(both, head_size, 1)
        low = lax.broadcasted_iota(jnp.int32, both.shape, 1) < head_size
        key_head, g = 2 * at // group, 2 * at % group
        pair, side = key_head // 2, key_head % 2
        for extra in range(2):
            source = both if extra == side else swapped
            kept_lanes = jnp.where(low if side == 0 else jnp.logical_not(low), source, 0.0)
            first = (side * group + g + extra) * tok
            q_ref[pair, first:first + tok, :] = kept_lanes.astype(jnp.bfloat16)
    own[KV].start()
    early = [(kind, step) for step in range(n) for kind in (GATE, UP)]
    blocks = pairs * per_pair
    done_blocks = 0
    for slot, (kind, step) in enumerate(early):
        if slot < n:
            serve(KV, slot)
        if slot > 0:
            serve(kind, step)
        if slot == 1:
            give_wo.start()
        if slot == 2 * n - 3:
            for ahead in (LOW, HIGH):
                serve(ahead, 0)
        if slot == n:
            own[KV].wait()
            sibling_gave(KV, range(n))
        if slot >= n:
            target = min(blocks, -(-blocks * (slot - n + 1) // (n - 2)))
            while done_blocks < target:
                attend(done_blocks)
                done_blocks += 1
        if slot == 2 * n - 3:
            assemble()
        if slot == 2 * n - 2:
            give_context.start()
        if slot == 2 * n - 1:
            normalize()
    tiles = units // tile
    fed = 0
    feed_from, feed_slots = 5, n - 5
    stage_of = {n // 2 + i: ([n // 2 - i, n // 2 + i] if i else [n // 2]) for i in range(n // 2)}
    waiting = []
    late = [(kind, step) for step in range(n) for kind in (LOW, HIGH)]
    for slot, (kind, step) in enumerate(late):
        if step > 0:
            serve(kind, step)
        for d in waiting:
            give_terms(d).start()
        waiting = []
        if slot == 2:
            give_normed.start()
            for other in (GATE, UP):
                own[other].wait()
                sibling_gave(other, range(n))
        if slot == feed_from - 1:
            take_normed.wait_recv()
        if feed_from - 1 <= slot < n:
            target = min(tiles, -(-tiles * (slot - feed_from + 2) // (feed_slots + 1)))
            if target > fed:
                feed(fed, target)
                fed = target
        if slot == n:
            own[3].wait()
            for other in (LOW, HIGH):
                sibling_gave(other, range(1))
            lower(0)
            waiting.append(0)
        if kind == HIGH and step >= n // 2:
            fresh = range(1, step + 1) if step == n // 2 else range(step, step + 1)
            for other in (LOW, HIGH):
                sibling_gave(other, fresh)
            for d in stage_of[step]:
                lower(d)
                waiting.append(d)
    give_terms(waiting[0]).start()
    ready = [0] + [d for step in range(n // 2, n - 1) for d in stage_of[step]]
    for d in ready:
        emit(d)
    give_terms(waiting[1]).start()
    for d in waiting:
        emit(d)
    for kind in range(5):
        for step in range(n):
            for way in range(2):
                if step < n - 1:
                    ring(kind, step, way).wait_send()
                across(kind, step, way).wait_send()
    give_context.wait_send()
    give_wo.wait_send()
    give_normed.wait_send()
    for d in range(n):
        give_terms(d).wait_send()


def fast_body(depth, queries, keys, values, q_gain, k_gain, w_out, residual, norm_gain, w_gate, w_up, w_down):
    tok_rows = queries.shape[0]
    head_size = q_gain.shape[0]
    q_heads = queries.shape[1] // head_size
    kv_heads = keys.shape[1] // head_size
    q_group = q_heads // kv_heads
    n_sp = 4 * depth
    positions = lax.axis_index("sp") * tok_rows + jnp.arange(tok_rows, dtype=jnp.int32)
    half_size = head_size // 2
    inv_freq = THETA ** (-jnp.arange(0, half_size, 2, dtype=jnp.float32) / half_size)
    row_angle = (positions // GRID_W).astype(jnp.float32)[:, None] * inv_freq[None, :]
    col_angle = (positions % GRID_W).astype(jnp.float32)[:, None] * inv_freq[None, :]
    angle = jnp.concatenate([row_angle, row_angle, col_angle, col_angle] * 2, axis=1)
    cos_table, sin_table = jnp.cos(angle), jnp.sin(angle)
    pairs = kv_heads // 2
    padded = (pairs, 2 * q_group * tok_rows, 2 * head_size)
    kv_shape = (tok_rows, keys.shape[1] + values.shape[1])
    tokens = n_sp * tok_rows
    any_space = pl.BlockSpec(memory_space=pl.ANY)
    vmem = pl.BlockSpec(memory_space=pltpu.VMEM)
    n = 2 * depth
    own_count, width = residual.shape
    depth_in, units = w_gate.shape
    lanes_down = w_down.shape[1]
    bf16, f32 = jnp.bfloat16, jnp.float32
    return pl.pallas_call(
        functools.partial(layer_kernel, depth, head_size),
        out_shape=jax.ShapeDtypeStruct(residual.shape, bf16),
        in_specs=[vmem] * 9 + [any_space] * 4,
        out_specs=vmem,
        scratch_shapes=[
            pltpu.VMEM(padded, bf16),
            pltpu.VMEM(kv_shape, bf16),
            pltpu.VMEM((tokens, kv_shape[1]), bf16),
            pltpu.VMEM((n_sp * depth_in, units), bf16),
            pltpu.VMEM((n_sp * depth_in, units), bf16),
            pltpu.VMEM((units, n_sp * lanes_down), bf16),
            pltpu.VMEM(w_out.shape, bf16),
            pltpu.VMEM(w_out.shape, bf16),
            pltpu.VMEM(padded, bf16),
            pltpu.VMEM(queries.shape, bf16),
            pltpu.VMEM((own_count, queries.shape[1]), bf16),
            pltpu.VMEM((own_count, width), f32),
            pltpu.VMEM((tok_rows, width), bf16),
            pltpu.VMEM((tok_rows, units), bf16),
            pltpu.VMEM((tok_rows, 2 * lanes_down), f32),
            pltpu.VMEM((n, own_count, 2 * lanes_down), f32),
            pltpu.VMEM((n, own_count, 2 * lanes_down), bf16),
            pltpu.VMEM((n, own_count, 2 * lanes_down), bf16),
            pltpu.SemaphoreType.DMA((5,)),
            pltpu.SemaphoreType.DMA((5, n - 1, 2)),
            pltpu.SemaphoreType.DMA((5, n - 1, 2)),
            pltpu.SemaphoreType.DMA((5, n, 2)),
            pltpu.SemaphoreType.DMA((5, n, 2)),
            pltpu.SemaphoreType.DMA((3 + n,)),
            pltpu.SemaphoreType.DMA((3 + n,)),
        ],
        compiler_params=pltpu.CompilerParams(
            collective_id=0, has_side_effects=True, vmem_limit_bytes=63 * 1024 * 1024
        ),
        name="layer",
    )(
        queries, keys, values, q_gain[None, :], k_gain[None, :], cos_table, sin_table,
        residual, norm_gain[None, :], w_out, w_gate, w_up, w_down)


def solution(mesh):
    depth = physical_ring(mesh)
    inner = body if depth is None else functools.partial(fast_body, depth)
    return jax.shard_map(
        inner,
        mesh=mesh,
        in_specs=(
            P("sp", "tp"),
            P("sp", "tp"),
            P("sp", "tp"),
            P(),
            P(),
            P("tp", None),
            P(("sp", "tp"), None),
            P(),
            P("sp", "tp"),
            P("sp", "tp"),
            P("tp", "sp"),
        ),
        out_specs=P(("sp", "tp"), None),
        check_vma=False,
    )
```

profile of v0, /device:TPU:0, one launch (start us, length us, event | category | flops | bytes accessed | tf_op | source)
XLA Modules:
  0.0 197.3 jit_solution(5867320484518702156)
XLA Ops:
  0.0 0.1 broadcast_multiply_fusion
  0.2 0.3 concatenate.3
  0.4 1.0 fusion.3
  1.4 194.1 %layer.1 = bf16[96,2048]{1,0:T(8,128)(2,1)} custom-call(bf16[192,512]{1,0:T(8,128)(2,1)} %raw_q.1, bf16[192,256]{1,0:T(8,128)(2,1)} %raw_k.1, bf16[192,256]{1,0:T(8,128)(2,1)} %raw_v.1, f32[1,64]{1,0:T(1,128)} %bitcast.4, f32[1,64]{1,0:T(1,128)} %bitcast.5, f32[192,128]{1,0:T(8,128)} %get-tuple-element.6.cos_ref, f32[192,128]{1,0:T(8,128)} %get-tuple-element.5.sin_ref, ...), custom_call_target="tpu_custom_call" | custom-call | tf_op jit(solution)/shard_map/layer/pallas_call | solution.py:524
  195.6 1.8 copy.13
  (2 shorter events, 0.0 us)
where the time goes:
time: 198 us; the launch traced here: 197 us
  Pallas kernels  194 us (98%)
  local copies, waits for them, and re-layouts  3.04 us (2%)
    pallas_call x1, Pallas kernels, fast_body(): pl.pallas_call(functools.partial(layer_kernel, depth, head_size), out_sha...  194 us

commit v1 on v0

v1 whole, which is shorter than its diff:
```python
import functools
import math

import jax
import jax.numpy as jnp
from jax import lax
from jax.experimental import pallas as pl
from jax.experimental.pallas import tpu as pltpu
from jax.sharding import PartitionSpec as P

GRID_W = 128


EPS = 1e-06
THETA = 10000.0


def turn_half(part, angle):
    quarter = part.shape[-1] // 2
    cos_table = jnp.cos(angle)[:, None, :]
    sin_table = jnp.sin(angle)[:, None, :]
    first_part = part[..., :quarter]
    second_part = part[..., quarter:]
    return jnp.concatenate(
        [
            first_part * cos_table - second_part * sin_table,
            first_part * sin_table + second_part * cos_table,
        ],
        axis=-1,
    )


def head_norm_rope(flat, gain, offset, head_count):
    tok_rows = flat.shape[0]
    head_size = flat.shape[1] // head_count
    heads = flat.astype(jnp.float32).reshape(tok_rows, head_count, head_size)
    heads = heads * lax.rsqrt(jnp.mean(heads * heads, axis=-1, keepdims=True) + EPS) * gain
    positions = offset + jnp.arange(tok_rows, dtype=jnp.int32)
    row_pos = (positions // GRID_W).astype(jnp.float32)
    col_pos = (positions % GRID_W).astype(jnp.float32)
    half_size = head_size // 2
    inv_freq = THETA ** (-jnp.arange(0, half_size, 2, dtype=jnp.float32) / half_size)
    turned = jnp.concatenate(
        [
            turn_half(heads[..., :half_size], row_pos[:, None] * inv_freq[None, :]),
            turn_half(heads[..., half_size:], col_pos[:, None] * inv_freq[None, :]),
        ],
        axis=-1,
    )
    return turned.reshape(tok_rows, head_count * head_size).astype(jnp.bfloat16)


def body(queries, keys, values, q_gain, k_gain, w_out, residual, norm_gain, w_gate, w_up, w_down):
    tok_rows = queries.shape[0]
    head_size = q_gain.shape[0]
    q_heads = queries.shape[1] // head_size
    kv_heads = keys.shape[1] // head_size
    q_group = q_heads // kv_heads
    offset = lax.axis_index("sp") * tok_rows
    q_rot = head_norm_rope(queries, q_gain, offset, q_heads)
    k_rot = head_norm_rope(keys, k_gain, offset, kv_heads)
    query_groups = q_rot.reshape(tok_rows, kv_heads, q_group, head_size)
    score_scale = head_size ** (-0.5)
    start_state = (
        jnp.full((kv_heads, q_group, tok_rows), -1e30, jnp.float32),
        jnp.zeros((kv_heads, q_group, tok_rows), jnp.float32),
        jnp.zeros((kv_heads, q_group, tok_rows, head_size), jnp.float32),
    )
    running = start_state
    key_piece = lax.all_gather(k_rot, "sp", axis=0, tiled=True)
    value_piece = lax.all_gather(values, "sp", axis=0, tiled=True)
    piece_len = key_piece.shape[0]
    block_len = math.gcd(piece_len, 512)
    blocks = piece_len // block_len
    key_blocks = key_piece.reshape(blocks, block_len, kv_heads, head_size)
    value_blocks = value_piece.reshape(blocks, block_len, kv_heads, head_size)

    def update(state, block_pair):
        prior_max, totals, accum = state
        key_block, value_block = block_pair
        scores = (
            jnp.einsum(
                "qhgd,khd->hgqk", query_groups, key_block, preferred_element_type=jnp.float32
            )
            * score_scale
        )
        new_max = jnp.maximum(prior_max, jnp.max(scores, axis=-1))
        weights = jnp.exp(scores - new_max[..., None])
        factor = jnp.exp(prior_max - new_max)
        totals = totals * factor + jnp.sum(weights, axis=-1)
        accum = accum * factor[..., None] + jnp.einsum(
            "hgqk,khd->hgqd",
            weights.astype(jnp.bfloat16),
            value_block,
            preferred_element_type=jnp.float32,
        )
        return ((new_max, totals, accum), None)

    running, unused = lax.scan(update, running, (key_blocks, value_blocks))
    final_max, totals, accum = running
    mixed = accum / totals[..., None]
    attn = (
        jnp.transpose(mixed, (2, 0, 1, 3))
        .reshape(tok_rows, q_heads * head_size)
        .astype(jnp.bfloat16)
    )
    own_rows = lax.all_to_all(attn, "tp", split_axis=0, concat_axis=1, tiled=True)
    columns = own_rows
    proj = jnp.dot(
        columns, lax.all_gather(w_out, "tp", axis=0, tiled=True), preferred_element_type=jnp.float32
    )
    mid = residual.astype(jnp.float32) + proj
    normed = (
        mid * lax.rsqrt(jnp.mean(mid * mid, axis=-1, keepdims=True) + EPS) * norm_gain
    ).astype(jnp.bfloat16)
    gathered = lax.all_gather(normed, "tp", axis=0, tiled=True)
    columns = gathered
    gate = jnp.dot(
        columns,
        lax.all_gather(w_gate, "sp", axis=0, tiled=True),
        preferred_element_type=jnp.float32,
    )
    up_part = jnp.dot(
        columns, lax.all_gather(w_up, "sp", axis=0, tiled=True), preferred_element_type=jnp.float32
    )
    hidden = (jax.nn.silu(gate) * up_part).astype(jnp.bfloat16)
    terms = jnp.dot(
        hidden, lax.all_gather(w_down, "sp", axis=1, tiled=True), preferred_element_type=jnp.float32
    )
    down = lax.psum_scatter(
        terms.astype(jnp.bfloat16), "tp", scatter_dimension=0, tiled=True
    ).astype(jnp.float32)
    return (mid + 0.5 * down).astype(jnp.bfloat16)


MESH = pl.DeviceIdType.MESH
BLOCK = 128


def line_of_chips(mesh):
    count = mesh.shape["sp"]
    try:
        places = [(tuple(d.coords), d.core_on_chip) for d in mesh.devices[:, 0].flat]
    except AttributeError:
        return None
    if count % 4 or count < 12 or mesh.shape["tp"] != 2:
        return None
    first = places[0][0]
    for at, (coords, core) in enumerate(places):
        chip = at // 2
        want = (first[0], first[1] + chip % 2, first[2] + chip // 2)
        if coords != want or core != at % 2:
            return None
    return count // 4


def message_count(n):
    events = 2 * (n - 1)
    return 9 * (events + 1) + 2 * events + 12 * n + 3 + 4 * events + 6 * n + n + 2


def slab_width(units, n):
    blocks = units // BLOCK
    return -(-blocks // n) * BLOCK


def turned_heads(head_size, x_ref, g_ref, cos_ref, sin_ref):
    x = x_ref[...].astype(jnp.float32)
    width = x.shape[1]
    lane = lax.broadcasted_iota(jnp.int32, (width, width), 0) // head_size
    other = lax.broadcasted_iota(jnp.int32, (width, width), 1) // head_size
    same = (lane == other).astype(jnp.float32)
    mean = jnp.dot(
        x * x, same, preferred_element_type=jnp.float32, precision=lax.Precision.HIGHEST
    ) * (1.0 / head_size)
    h = x * lax.rsqrt(mean + EPS) * jnp.concatenate([g_ref[...]] * (width // head_size), axis=1)
    quarter = head_size // 4
    repeats = width // cos_ref.shape[1]
    cos_table = jnp.concatenate([cos_ref[...]] * repeats, axis=1)
    sin_table = jnp.concatenate([sin_ref[...]] * repeats, axis=1)
    at = lax.broadcasted_iota(jnp.int32, x.shape, 1)
    is_first = (at // quarter) % 2 == 0
    ahead = pltpu.roll(h, width - quarter, 1)
    behind = pltpu.roll(h, quarter, 1)
    turned = h * cos_table + jnp.where(is_first, -ahead, behind) * sin_table
    return turned.astype(jnp.bfloat16)


def when(condition, action):
    if condition is None:
        action()
    else:
        pl.when(condition)(action)


def both(one, other):
    if one is None:
        return other
    if other is None:
        return one
    return jnp.logical_and(one, other)


def layer_kernel(
    n, head_size,
    raw_q, raw_k, raw_v, qg_ref, kg_ref, cos_ref, sin_ref, res_ref, gain_ref, wo_in, wg_in, wu_in, wd_in,
    out_ref,
    q_ref, kv_all, wg_all, wu_all, wd_all, wo_own, wo_other, attn, context, context_in, mid, normed, hidden,
    part, leaving, line_in, pair_in, own_sem, send_sem, recv_sem,
):
    sp = lax.axis_index("sp")
    tp = lax.axis_index("tp")
    core = lax.rem(sp, 2)
    y = lax.rem(lax.div(sp, 2), 2)
    z = lax.div(sp, 4)

    def device(zz, yy, cc):
        return (zz * 2 + yy) * 2 + cc

    def wrapped(zz):
        return lax.rem(zz + n, n)

    sibling = (device(z, y, 1 - core), tp)
    across = (device(z, 1 - y, core), tp)
    partner = (sp, 1 - tp)

    def level(zz):
        return (device(zz, y, core), tp)

    barrier = pltpu.get_barrier_semaphore()
    greeted = [sibling, across, partner] + [level(wrapped(z + d)) for d in range(1, n)]
    for target in greeted:
        pl.semaphore_signal(barrier, inc=1, device_id=target, device_id_type=MESH)
    pl.semaphore_wait(barrier, len(greeted))

    slots = {}
    sent = []

    def message(key, src, dst, target):
        slot = slots.setdefault(key, len(slots))
        return pltpu.make_async_remote_copy(
            src_ref=src, dst_ref=dst, send_sem=send_sem.at[slot], recv_sem=recv_sem.at[slot],
            device_id=target, device_id_type=MESH,
        )

    def send(key, condition, src, dst, target):
        def make():
            return message(key, src(), dst(), target)

        when(condition, lambda: make().start())
        sent.append((condition, make))

    def land(key, condition, piece):
        when(condition, lambda: message(key, piece(), piece(), partner).wait_recv())

    arrivals = [[(s, w) for w in range(2)] for s in range(n - 1)]
    events = [None] + [e for step in arrivals for e in step]
    room = (z <= n - 2, z >= 1)
    ahead = (level(z + 1), level(z - 1))

    def home(e):
        if e is None:
            return z
        return z - 1 - e[0] if e[1] == 0 else z + 1 + e[0]

    def real(e):
        if e is None:
            return None
        return z >= e[0] + 1 if e[1] == 0 else z <= n - 2 - e[0]

    def pass_on(name, e, src, dst):
        for w in range(2) if e is None else (e[1],):
            step = 0 if e is None else e[0] + 1
            if step <= n - 2:
                send((name, step, w), both(real(e), room[w]), src, dst, ahead[w])

    tok = raw_q.shape[0]
    kv_width = raw_k.shape[1]

    def kv_piece(j, zz, yy, cc):
        start = pl.multiple_of(device(zz, yy, cc) * tok, tok)
        return kv_all.at[pl.ds(start, tok), j * kv_width:(j + 1) * kv_width]

    def kv_serve(j, e):
        def dst():
            return kv_piece(j, home(e), y, core)

        if e is not None:
            land((("kv", j), e[0], e[1]), real(e), dst)
        src = (lambda: raw_v) if e is None and j == 1 else dst
        pass_on(("kv", j), e, src, dst)
        send(("kv y", j, e), real(e), src, dst, across)
        send(("kv core", j, e, 0), real(e), src, dst, sibling)

    def kv_cross(j, e):
        def piece():
            return kv_piece(j, home(e), 1 - y, core)

        land(("kv y", j, e), real(e), piece)
        send(("kv core", j, e, 1), real(e), piece, piece, sibling)

    def kv_finish(j, e):
        land(("kv core", j, e, 0), real(e), lambda: kv_piece(j, home(e), y, 1 - core))
        land(("kv core", j, e, 1), real(e), lambda: kv_piece(j, home(e), 1 - y, 1 - core))

    GATE, UP, DOWN = range(3)
    weights_in = (wg_in, wu_in, wd_in)
    rows, units = wg_in.shape
    lanes_down = wd_in.shape[1]
    blocks = units // BLOCK
    slab = wg_all.shape[1]

    def first_block(zz):
        return lax.div(zz * blocks, n)

    def weight_in(k, zz):
        span = pl.ds(pl.multiple_of(first_block(zz) * BLOCK, BLOCK), slab)
        return wd_in.at[span, :] if k == DOWN else weights_in[k].at[:, span]

    def weight(k, zz, yy, cc):
        o = device(zz, yy, cc)
        if k == DOWN:
            return wd_all.at[:, pl.ds(pl.multiple_of(o * lanes_down, lanes_down), lanes_down)]
        return (wg_all, wu_all)[k].at[pl.ds(pl.multiple_of(o * rows, rows), rows), :]

    def weight_line(k, d):
        zt = wrapped(z + d)
        send(
            ("w z", k, d), None,
            lambda: weight_in(k, zt), lambda: weight(k, z, y, core), level(zt),
        )

    def weight_serve(k, d):
        zs = wrapped(z - d)

        def dst():
            return weight(k, zs, y, core)

        src = dst
        if d == 0:
            src = lambda: weight_in(k, z)
        else:
            land(("w z", k, d), None, dst)
        send(("w y", k, d), None, src, dst, across)
        send(("w core", k, d, 0), None, src, dst, sibling)

    def weight_cross(k, d):
        def piece():
            return weight(k, wrapped(z - d), 1 - y, core)

        land(("w y", k, d), None, piece)
        send(("w core", k, d, 1), None, piece, piece, sibling)

    own = [
        pltpu.make_async_copy(weight_in(k, z), weight(k, z, y, core), own_sem.at[k]) for k in range(3)
    ] + [pltpu.make_async_copy(wo_in, wo_own, own_sem.at[3])]

    def weight_finish(k):
        own[k].wait()
        for d in range(n):
            zs = wrapped(z - d)
            land(("w core", k, d, 0), None, lambda: weight(k, zs, y, 1 - core))
            land(("w core", k, d, 1), None, lambda: weight(k, zs, 1 - y, 1 - core))

    wo_half = wo_in.shape[0] // 2

    def wo_part(ref, cc):
        return ref.at[pl.ds(pl.multiple_of(cc * wo_half, wo_half), wo_half), :]

    pairs, q_rows, lanes = q_ref.shape
    block = math.gcd(q_rows, 256)
    per_pair = q_rows // block

    def attend(at):
        pair, which = at // per_pair, at % per_pair
        span = slice(which * block, (which + 1) * block)
        q = q_ref[pair, span, :]
        k = kv_all[:, pair * lanes:(pair + 1) * lanes]
        v = kv_all[:, (pairs + pair) * lanes:(pairs + pair + 1) * lanes]
        scores = lax.dot_general(
            q, k, (((1,), (1,)), ((), ())), preferred_element_type=jnp.float32
        )
        weights = jnp.exp(scores - jnp.max(scores, axis=-1, keepdims=True))
        total = jnp.sum(weights, axis=-1, keepdims=True)
        mixed = jnp.dot(weights.astype(jnp.bfloat16), v, preferred_element_type=jnp.float32)
        attn[pair, span, :] = (mixed / total).astype(jnp.bfloat16)

    def assemble():
        group = q_rows // (2 * tok)
        pieces = []
        for pair in range(pairs):
            for side in range(2):
                for g in range(0, group, 2):
                    lower = attn[pair, pl.ds((side * group + g) * tok, tok), :].astype(jnp.float32)
                    upper = attn[pair, pl.ds((side * group + g + 1) * tok, tok), :].astype(jnp.float32)
                    if side == 1:
                        lower = pltpu.roll(lower, head_size, 1)
                    else:
                        upper = pltpu.roll(upper, head_size, 1)
                    lane = lax.broadcasted_iota(jnp.int32, lower.shape, 1)
                    pieces.append(jnp.where(lane < head_size, lower, upper).astype(jnp.bfloat16))
        context[...] = jnp.concatenate(pieces, axis=1)

    own_count, width = res_ref.shape
    rows_of = own_count // 2
    mine = pl.ds(pl.multiple_of(tp * own_count, own_count), own_count)
    theirs = pl.ds(pl.multiple_of((1 - tp) * own_count, own_count), own_count)

    def span_of(zz, f):
        xx, part_of = ((tp, 0), (tp, 1), (1 - tp, 1), (1 - tp, 0))[f]
        start = ((zz * 2 + xx) * 2 + part_of) * rows_of
        return pl.ds(pl.multiple_of(start, rows_of), rows_of)

    def normalize():
        held, other = context[mine, :], context_in[...]
        wide = math.gcd(width, 512)
        for at in range(0, width, wide):
            cols = slice(at, at + wide)
            mid[:, cols] = res_ref[:, cols].astype(jnp.float32) + (
                jnp.dot(held, wo_own[:, cols], preferred_element_type=jnp.float32)
                + jnp.dot(other, wo_other[:, cols], preferred_element_type=jnp.float32)
            )
        value = mid[...]
        scale = lax.rsqrt(jnp.mean(value * value, axis=-1, keepdims=True) + EPS)
        result = (value * scale * gain_ref[...]).astype(jnp.bfloat16)
        normed[span_of(z, 0), :] = result[:rows_of]
        normed[span_of(z, 1), :] = result[rows_of:]

    def rows_serve(f, e):
        def piece():
            return normed.at[span_of(home(e), f), :]

        if e is not None:
            land((("rows", f), e[0], e[1]), real(e), piece)
        elif f == 2:
            land(("rows x", "second"), None, piece)
        pass_on(("rows", f), e, piece, piece)
        if f == 0:
            send(("rows x", e), real(e), piece, piece, partner)
        if f == 1 and e is None:
            send(("rows x", "second"), None, piece, piece, partner)

    def rows_cross(e):
        land(("rows x", e), real(e), lambda: normed.at[span_of(home(e), 3), :])

    def nearest(p):
        result = 0
        for zz in range(n):
            order = sorted(range(n), key=lambda other: (abs(other - zz), other))
            result = jnp.where(z == zz, order[p], result)
        return result

    piece_rows = 2 * own_count
    tile = math.gcd(slab, 256)
    valid = (first_block(z + 1) - first_block(z)) * BLOCK

    def feed(p):
        start = pl.multiple_of(nearest(p) * piece_rows, piece_rows)

        @pl.loop(0, slab // tile)
        def _(at):
            cols = pl.ds(pl.multiple_of(at * tile, tile), tile)
            x = normed[pl.ds(start, piece_rows), :]
            gate = jnp.dot(x, wg_all[:, cols], preferred_element_type=jnp.float32)
            up = jnp.dot(x, wu_all[:, cols], preferred_element_type=jnp.float32)
            unit = at * tile + lax.broadcasted_iota(jnp.int32, gate.shape, 1)
            product = jnp.where(unit < valid, gate / (1.0 + jnp.exp(-gate)) * up, 0.0)
            hidden[p * piece_rows:(p + 1) * piece_rows, cols] = product.astype(jnp.bfloat16)

    wide_down = math.gcd(width, 512)

    def lower(p):
        zz = nearest(p)
        start = pl.multiple_of(zz * piece_rows, piece_rows)

        @pl.loop(0, width // wide_down)
        def _(at):
            cols = pl.ds(pl.multiple_of(at * wide_down, wide_down), wide_down)
            part[pl.ds(start, piece_rows), cols] = jnp.dot(
                hidden[p * piece_rows:(p + 1) * piece_rows, :], wd_all[:, cols],
                preferred_element_type=jnp.float32,
            )

        leaving[span_of(zz, 3), :] = part[span_of(zz, 3), :].astype(jnp.bfloat16)
        send(
            ("sum x", p), None,
            lambda: leaving.at[span_of(zz, 3), :], lambda: pair_in.at[zz], partner,
        )

    def add(zz, f, ref):
        part[span_of(zz, f), :] = part[span_of(zz, f), :] + ref[...].astype(jnp.float32)

    def sum_send(f, w, d):
        zz = z + d if w == 0 else z - d
        inside = z <= n - 1 - d if w == 0 else z >= d
        if d < n - 1:
            def take():
                message(("sum", f, w, d + 1), line_in.at[f, w, d], line_in.at[f, w, d], partner).wait_recv()
                add(zz, f, line_in.at[f, w, d])

            when(both(inside, room[1 - w]), take)

        def put():
            leaving[span_of(zz, f), :] = part[span_of(zz, f), :].astype(jnp.bfloat16)

        when(inside, put)
        send(
            ("sum", f, w, d), inside,
            lambda: leaving.at[span_of(zz, f), :], lambda: line_in.at[f, w, d - 1], ahead[w],
        )

    def sum_finish(f):
        for w in range(2):
            def take():
                message(("sum", f, w, 1), line_in.at[f, w, 0], line_in.at[f, w, 0], partner).wait_recv()
                add(z, f, line_in.at[f, w, 0])

            when(room[1 - w], take)

    for copy in own:
        copy.start()
    kv_serve(1, None)
    send(
        ("wo", 0), None, lambda: wo_part(wo_in, core), lambda: wo_part(wo_other, core), partner
    )
    weight_line(GATE, 1)
    own_rows = pl.ds(pl.multiple_of(sp * tok, tok), tok)
    kv_all[own_rows, :kv_width] = turned_heads(head_size, raw_k, kg_ref, cos_ref, sin_ref)
    kv_all[own_rows, kv_width:] = raw_v[...]
    kv_serve(0, None)
    turned = turned_heads(head_size, raw_q, qg_ref, cos_ref, sin_ref).astype(jnp.float32)
    turned = turned * head_size ** (-0.5)
    group = q_rows // (2 * tok)
    for at in range(raw_q.shape[1] // lanes):
        together = turned[:, at * lanes:(at + 1) * lanes]
        swapped = pltpu.roll(together, head_size, 1)
        low = lax.broadcasted_iota(jnp.int32, together.shape, 1) < head_size
        key_head, g = 2 * at // group, 2 * at % group
        pair, side = key_head // 2, key_head % 2
        for extra in range(2):
            source = together if extra == side else swapped
            kept_lanes = jnp.where(low if side == 0 else jnp.logical_not(low), source, 0.0)
            first = (side * group + g + extra) * tok
            q_ref[pair, first:first + tok, :] = kept_lanes.astype(jnp.bfloat16)

    lines = [(k, d) for k in range(3) for d in range(1, n)][1:]
    crossing = [None]
    for step in arrivals:
        for j in (1, 0):
            for e in step:
                kv_serve(j, e)
        weight_line(*lines.pop(0))
        for j in (1, 0):
            for e in crossing:
                kv_cross(j, e)
        crossing = step
    for k, d in lines:
        weight_line(k, d)
    weight_serve(GATE, 0)
    for j in (1, 0):
        for e in crossing:
            kv_cross(j, e)
    for j in (1, 0):
        for e in events:
            kv_finish(j, e)

    tasks = []
    served = [(k, d) for k in range(3) for d in range(n)]
    for at in range(1, len(served)):
        tasks.append((weight_serve, served[at]))
        tasks.append((weight_cross, served[at - 1]))
    tasks.append((weight_cross, served[-1]))

    def work(count):
        for _ in range(min(count, len(tasks))):
            task, what = tasks.pop(0)
            task(*what)

    for at in range(pairs * per_pair):
        attend(at)
        work(2)
        if at == 2:
            land(("wo", 0), None, lambda: wo_part(wo_other, core))
            send(
                ("wo", 1), None,
                lambda: wo_part(wo_other, core), lambda: wo_part(wo_other, core), sibling,
            )
    assemble()
    work(1)
    send(("context",), None, lambda: context.at[theirs, :], lambda: context_in, partner)
    work(1)
    land(("wo", 1), None, lambda: wo_part(wo_other, 1 - core))
    own[3].wait()
    land(("context",), None, lambda: context_in)
    normalize()
    work(1)
    for f in (0, 1):
        rows_serve(f, None)
    work(1)
    rows_serve(2, None)
    rows_cross(None)
    work(len(tasks))
    weight_finish(GATE)
    weight_finish(UP)
    feed(0)
    for at, step in enumerate(arrivals):
        for f in range(3):
            for e in step:
                rows_serve(f, e)
        if at == 0:
            weight_finish(DOWN)
            lower(0)
        for e in step:
            rows_cross(e)
        feed(at + 1)
        lower(at + 1)
    for p in range(n):
        zz = nearest(p)
        land(("sum x", p), None, lambda: pair_in.at[zz])
        add(zz, 0, pair_in.at[zz])
    for d in range(n - 1, 0, -1):
        for f in (1, 2, 0):
            for w in range(2):
                sum_send(f, w, d)
    sum_finish(2)
    leaving[span_of(z, 2), :] = part[span_of(z, 2), :].astype(jnp.bfloat16)
    sum_finish(0)
    out_ref[:rows_of, :] = (mid[:rows_of, :] + 0.5 * part[span_of(z, 0), :]).astype(jnp.bfloat16)
    send(("sum x", "second"), None, lambda: leaving.at[span_of(z, 2), :], lambda: pair_in.at[n], partner)
    sum_finish(1)
    land(("sum x", "second"), None, lambda: pair_in.at[n])
    add(z, 1, pair_in.at[n])
    out_ref[rows_of:, :] = (mid[rows_of:, :] + 0.5 * part[span_of(z, 1), :]).astype(jnp.bfloat16)
    for condition, make in sent:
        when(condition, lambda: make().wait_send())
    assert len(slots) <= send_sem.shape[0]


def fast_body(n, queries, keys, values, q_gain, k_gain, w_out, residual, norm_gain, w_gate, w_up, w_down):
    tok_rows = queries.shape[0]
    head_size = q_gain.shape[0]
    q_heads = queries.shape[1] // head_size
    kv_heads = keys.shape[1] // head_size
    q_group = q_heads // kv_heads
    n_sp = 4 * n
    positions = lax.axis_index("sp") * tok_rows + jnp.arange(tok_rows, dtype=jnp.int32)
    half_size = head_size // 2
    inv_freq = THETA ** (-jnp.arange(0, half_size, 2, dtype=jnp.float32) / half_size)
    row_angle = (positions // GRID_W).astype(jnp.float32)[:, None] * inv_freq[None, :]
    col_angle = (positions % GRID_W).astype(jnp.float32)[:, None] * inv_freq[None, :]
    angle = jnp.concatenate([row_angle, row_angle, col_angle, col_angle] * 2, axis=1)
    cos_table, sin_table = jnp.cos(angle), jnp.sin(angle)
    pairs = kv_heads // 2
    padded = (pairs, 2 * q_group * tok_rows, 2 * head_size)
    kv_width = keys.shape[1] + values.shape[1]
    tokens = n_sp * tok_rows
    any_space = pl.BlockSpec(memory_space=pl.ANY)
    vmem = pl.BlockSpec(memory_space=pltpu.VMEM)
    own_count, width = residual.shape
    depth_in, units = w_gate.shape
    lanes_down = w_down.shape[1]
    slab = slab_width(units, n)
    group_rows = 2 * n * own_count
    bf16, f32 = jnp.bfloat16, jnp.float32
    return pl.pallas_call(
        functools.partial(layer_kernel, n, head_size),
        out_shape=jax.ShapeDtypeStruct(residual.shape, bf16),
        in_specs=[vmem] * 9 + [any_space] * 4,
        out_specs=vmem,
        scratch_shapes=[
            pltpu.VMEM(padded, bf16),
            pltpu.VMEM((tokens, kv_width), bf16),
            pltpu.VMEM((n_sp * depth_in, slab), bf16),
            pltpu.VMEM((n_sp * depth_in, slab), bf16),
            pltpu.VMEM((slab, n_sp * lanes_down), bf16),
            pltpu.VMEM(w_out.shape, bf16),
            pltpu.VMEM(w_out.shape, bf16),
            pltpu.VMEM(padded, bf16),
            pltpu.VMEM(queries.shape, bf16),
            pltpu.VMEM((own_count, queries.shape[1]), bf16),
            pltpu.VMEM((own_count, width), f32),
            pltpu.VMEM((group_rows, width), bf16),
            pltpu.VMEM((group_rows, slab), bf16),
            pltpu.VMEM((group_rows, width), f32),
            pltpu.VMEM((group_rows, width), bf16),
            pltpu.VMEM((3, 2, n - 1, own_count // 2, width), bf16),
            pltpu.VMEM((n + 1, own_count // 2, width), bf16),
            pltpu.SemaphoreType.DMA((4,)),
            pltpu.SemaphoreType.DMA((message_count(n),)),
            pltpu.SemaphoreType.DMA((message_count(n),)),
        ],
        compiler_params=pltpu.CompilerParams(
            collective_id=0, has_side_effects=True, vmem_limit_bytes=63 * 1024 * 1024
        ),
        name="layer",
    )(
        queries, keys, values, q_gain[None, :], k_gain[None, :], cos_table, sin_table,
        residual, norm_gain[None, :], w_out, w_gate, w_up, w_down)


def solution(mesh):
    n = line_of_chips(mesh)
    inner = body if n is None else functools.partial(fast_body, n)
    return jax.shard_map(
        inner,
        mesh=mesh,
        in_specs=(
            P("sp", "tp"),
            P("sp", "tp"),
            P("sp", "tp"),
            P(),
            P(),
            P("tp", None),
            P(("sp", "tp"), None),
            P(),
            P("sp", "tp"),
            P("sp", "tp"),
            P("tp", "sp"),
        ),
        out_specs=P(("sp", "tp"), None),
        check_vma=False,
    )
```

time: 198 us -> 183 us (0.924)
  the two profiles are of different devices: /device:TPU:0 before, /device:TPU:18 now
where the time goes in v1:
time: 183 us
  Pallas kernels  180 us (98%)
  local copies, waits for them, and re-layouts  3.04 us (2%)
    pallas_call x1, Pallas kernels, fast_body(): pl.pallas_call(functools.partial(layer_kernel, n, head_size), out_shape=j...  180 us

profile of v1, /device:TPU:18, one launch (start us, length us, event | category | flops | bytes accessed | tf_op | source)
XLA Modules:
  0.0 183.0 jit_solution(9090958970926969363)
XLA Ops:
  0.0 0.1 broadcast_multiply_fusion
  0.2 0.3 concatenate.3
  0.4 1.0 fusion.3
  1.4 179.8 %layer.1 = bf16[96,2048]{1,0:T(8,128)(2,1)} custom-call(bf16[192,512]{1,0:T(8,128)(2,1)} %raw_q.1, bf16[192,256]{1,0:T(8,128)(2,1)} %raw_k.1, bf16[192,256]{1,0:T(8,128)(2,1)} %raw_v.1, f32[1,64]{1,0:T(1,128)} %bitcast.4, f32[1,64]{1,0:T(1,128)} %bitcast.5, f32[192,128]{1,0:T(8,128)} %get-tuple-element.6.cos_ref, f32[192,128]{1,0:T(8,128)} %get-tuple-element.5.sin_ref, ...), custom_call_target="tpu_custom_call" | custom-call | tf_op jit(solution)/shard_map/layer/pallas_call | solution.py:665
  181.2 1.8 copy.13
  (2 shorter events, 0.0 us)

commit v2 on v1

--- a/solution.py
+++ b/solution.py
@@ -156,12 +156,8 @@
 
 def message_count(n):
     events = 2 * (n - 1)
-    return 9 * (events + 1) + 2 * events + 12 * n + 3 + 4 * events + 6 * n + n + 2
-
-
-def slab_width(units, n):
-    blocks = units // BLOCK
-    return -(-blocks // n) * BLOCK
+    keys = 2 * events + 6 * (events + 1)
+    return keys + 27 * n + 1 + 2 * events + 8 * n
 
 
 def turned_heads(head_size, x_ref, g_ref, cos_ref, sin_ref):
@@ -205,8 +201,8 @@
     n, head_size,
     raw_q, raw_k, raw_v, qg_ref, kg_ref, cos_ref, sin_ref, res_ref, gain_ref, wo_in, wg_in, wu_in, wd_in,
     out_ref,
-    q_ref, kv_all, wg_all, wu_all, wd_all, wo_own, wo_other, attn, context, context_in, mid, normed, hidden,
-    part, leaving, line_in, pair_in, own_sem, send_sem, recv_sem,
+    q_ref, kv_all, wg_all, wu_all, wd_all, wo_own, attn, context, proj_out, proj_in, mid, normed, hidden,
+    part, leaving, line_in, own_sem, send_sem, recv_sem,
 ):
     sp = lax.axis_index("sp")
     tp = lax.axis_index("tp")
@@ -237,7 +233,9 @@
     sent = []
 
     def message(key, src, dst, target):
-        slot = slots.setdefault(key, len(slots))
+        slot = key
+        if isinstance(key, tuple):
+            slot = slots.setdefault(key, 3 * n + len(slots))
         return pltpu.make_async_remote_copy(
             src_ref=src, dst_ref=dst, send_sem=send_sem.at[slot], recv_sem=recv_sem.at[slot],
             device_id=target, device_id_type=MESH,
@@ -252,6 +250,14 @@
 
     def land(key, condition, piece):
         when(condition, lambda: message(key, piece(), piece(), partner).wait_recv())
+
+    near = [z]
+    for p in range(1, n):
+        level_at = 0
+        for zz in range(n):
+            order = sorted(range(n), key=lambda other: (abs(other - zz), -abs(2 * other - n + 1)))
+            level_at = jnp.where(z == zz, order[p], level_at)
+        near.append(level_at)
 
     arrivals = [[(s, w) for w in range(2)] for s in range(n - 1)]
     events = [None] + [e for step in arrivals for e in step]
@@ -307,65 +313,107 @@
     weights_in = (wg_in, wu_in, wd_in)
     rows, units = wg_in.shape
     lanes_down = wd_in.shape[1]
-    blocks = units // BLOCK
     slab = wg_all.shape[1]
-
-    def first_block(zz):
-        return lax.div(zz * blocks, n)
-
-    def weight_in(k, zz):
-        span = pl.ds(pl.multiple_of(first_block(zz) * BLOCK, BLOCK), slab)
+    share = slab // BLOCK
+
+    def first_block(zz, xx):
+        return lax.div(zz * share + xx, 2)
+
+    def unit_forms(zz, xx):
+        if share % 2 == 0:
+            return [(None, share // 2)]
+        many = lax.rem(zz + xx, 2) == 1
+        return [(jnp.logical_not(many), share // 2), (many, share // 2 + 1)]
+
+    def weight_in(k, zz, count):
+        span = pl.ds(pl.multiple_of(first_block(zz, tp) * BLOCK, BLOCK), count * BLOCK)
         return wd_in.at[span, :] if k == DOWN else weights_in[k].at[:, span]
 
-    def weight(k, zz, yy, cc):
+    def weight(k, xx, zz, yy, cc, keeper, count):
         o = device(zz, yy, cc)
+        before = xx * (first_block(keeper + 1, 0) - first_block(keeper, 0))
+        units_of = pl.ds(pl.multiple_of(before * BLOCK, BLOCK), count * BLOCK)
         if k == DOWN:
-            return wd_all.at[:, pl.ds(pl.multiple_of(o * lanes_down, lanes_down), lanes_down)]
-        return (wg_all, wu_all)[k].at[pl.ds(pl.multiple_of(o * rows, rows), rows), :]
-
-    def weight_line(k, d):
-        zt = wrapped(z + d)
-        send(
-            ("w z", k, d), None,
-            lambda: weight_in(k, zt), lambda: weight(k, z, y, core), level(zt),
+            return wd_all.at[units_of, pl.ds(pl.multiple_of(o * lanes_down, lanes_down), lanes_down)]
+        return (wg_all, wu_all)[k].at[pl.ds(pl.multiple_of(o * rows, rows), rows), units_of]
+
+    def weight_line(k, p):
+        zt = near[p]
+        for condition, count in unit_forms(zt, tp):
+            send(
+                k * n + wrapped(zt - z), condition,
+                functools.partial(weight_in, k, zt, count),
+                functools.partial(weight, k, tp, z, y, core, zt, count), level(zt),
+            )
+
+    def by_x(k, p):
+        return (p % 4 != 3, p % 2 == 0, p % 2 == 1)[k]
+
+    def weight_move(k, p, xx, yy, way):
+        target = {"x": partner, "y": across, "core": sibling}[way]
+        corner = (xx is not tp, yy is not y)
+        for condition, count in unit_forms(z, xx):
+            dst = functools.partial(weight, k, xx, near[p], yy, core, z, count)
+            src = dst
+            if p == 0 and corner == (False, False):
+                src = functools.partial(weight_in, k, z, count)
+            send(("w", way, k, p, corner), condition, src, dst, target)
+
+    other_x, other_y = 1 - tp, 1 - y
+
+    def weight_take(key, k, p, xx, yy, cc):
+        for condition, count in unit_forms(z, xx):
+            land(key, condition, functools.partial(weight, k, xx, near[p], yy, cc, z, count))
+
+    def weight_land(k, p, way, xx, yy):
+        corner = (xx is not tp, yy is not y)
+        seen = {"x": (not corner[0], corner[1]), "y": (corner[0], not corner[1])}[way]
+        weight_take(("w", way, k, p, seen), k, p, xx, yy, core)
+
+    def weight_arrive(k, p):
+        weight_take(k * n + wrapped(z - near[p]), k, p, tp, y, core)
+
+    def weight_serve(k, p):
+        if p > 0:
+            weight_arrive(k, p)
+        weight_move(k, p, tp, y, "y")
+        weight_move(k, p, tp, y, "x")
+        weight_move(k, p, tp, y, "core")
+
+    def cross_y(k, p):
+        weight_land(k, p, "y", tp, other_y)
+        if by_x(k, p):
+            weight_move(k, p, tp, other_y, "x")
+        weight_move(k, p, tp, other_y, "core")
+
+    def cross_x(k, p):
+        weight_land(k, p, "x", other_x, y)
+        if not by_x(k, p):
+            weight_move(k, p, other_x, y, "y")
+        weight_move(k, p, other_x, y, "core")
+
+    def cross_both(k, p):
+        weight_land(k, p, "x" if by_x(k, p) else "y", other_x, other_y)
+        weight_move(k, p, other_x, other_y, "core")
+
+    def own_copy(k, count):
+        return pltpu.make_async_copy(
+            weight_in(k, z, count), weight(k, tp, z, y, core, z, count), own_sem.at[k]
         )
 
-    def weight_serve(k, d):
-        zs = wrapped(z - d)
-
-        def dst():
-            return weight(k, zs, y, core)
-
-        src = dst
-        if d == 0:
-            src = lambda: weight_in(k, z)
-        else:
-            land(("w z", k, d), None, dst)
-        send(("w y", k, d), None, src, dst, across)
-        send(("w core", k, d, 0), None, src, dst, sibling)
-
-    def weight_cross(k, d):
-        def piece():
-            return weight(k, wrapped(z - d), 1 - y, core)
-
-        land(("w y", k, d), None, piece)
-        send(("w core", k, d, 1), None, piece, piece, sibling)
-
-    own = [
-        pltpu.make_async_copy(weight_in(k, z), weight(k, z, y, core), own_sem.at[k]) for k in range(3)
-    ] + [pltpu.make_async_copy(wo_in, wo_own, own_sem.at[3])]
-
-    def weight_finish(k):
-        own[k].wait()
-        for d in range(n):
-            zs = wrapped(z - d)
-            land(("w core", k, d, 0), None, lambda: weight(k, zs, y, 1 - core))
-            land(("w core", k, d, 1), None, lambda: weight(k, zs, 1 - y, 1 - core))
-
-    wo_half = wo_in.shape[0] // 2
-
-    def wo_part(ref, cc):
-        return ref.at[pl.ds(pl.multiple_of(cc * wo_half, wo_half), wo_half), :]
+    def own_each(act):
+        for k in range(3):
+            for condition, count in unit_forms(z, tp):
+                when(condition, lambda: act(own_copy(k, count)))
+
+    own_wo = pltpu.make_async_copy(wo_in, wo_own, own_sem.at[3])
+
+    def weight_finish(k, sides):
+        for p in range(n):
+            for xx in (tp, other_x):
+                for yy in sides:
+                    corner = (xx is not tp, yy is not y)
+                    weight_take(("w", "core", k, p, corner), k, p, xx, yy, 1 - core)
 
     pairs, q_rows, lanes = q_ref.shape
     block = math.gcd(q_rows, 256)
@@ -406,89 +454,84 @@
     mine = pl.ds(pl.multiple_of(tp * own_count, own_count), own_count)
     theirs = pl.ds(pl.multiple_of((1 - tp) * own_count, own_count), own_count)
 
-    def span_of(zz, f):
-        xx, part_of = ((tp, 0), (tp, 1), (1 - tp, 1), (1 - tp, 0))[f]
-        start = ((zz * 2 + xx) * 2 + part_of) * rows_of
-        return pl.ds(pl.multiple_of(start, rows_of), rows_of)
-
-    def normalize():
-        held, other = context[mine, :], context_in[...]
-        wide = math.gcd(width, 512)
+    def whole(zz):
+        return pl.ds(pl.multiple_of(zz * own_count, own_count), own_count)
+
+    def rows_at(zz, f):
+        return pl.ds(pl.multiple_of((zz * 2 + f) * rows_of, rows_of), rows_of)
+
+    wide = math.gcd(width, 512)
+
+    def project():
+        given = context[theirs, :]
         for at in range(0, width, wide):
             cols = slice(at, at + wide)
-            mid[:, cols] = res_ref[:, cols].astype(jnp.float32) + (
-                jnp.dot(held, wo_own[:, cols], preferred_element_type=jnp.float32)
-                + jnp.dot(other, wo_other[:, cols], preferred_element_type=jnp.float32)
+            proj_out[:, cols] = jnp.dot(
+                given, wo_own[:, cols], preferred_element_type=jnp.float32
+            ).astype(jnp.bfloat16)
+
+    def project_own():
+        held = context[mine, :]
+        for at in range(0, width, wide):
+            cols = slice(at, at + wide)
+            mid[:, cols] = res_ref[:, cols].astype(jnp.float32) + jnp.dot(
+                held, wo_own[:, cols], preferred_element_type=jnp.float32
             )
-        value = mid[...]
+
+    def normalize():
+        value = mid[...] + proj_in[...].astype(jnp.float32)
+        mid[...] = value
         scale = lax.rsqrt(jnp.mean(value * value, axis=-1, keepdims=True) + EPS)
-        result = (value * scale * gain_ref[...]).astype(jnp.bfloat16)
-        normed[span_of(z, 0), :] = result[:rows_of]
-        normed[span_of(z, 1), :] = result[rows_of:]
+        normed[whole(z), :] = (value * scale * gain_ref[...]).astype(jnp.bfloat16)
 
     def rows_serve(f, e):
         def piece():
-            return normed.at[span_of(home(e), f), :]
+            return normed.at[rows_at(home(e), f), :]
 
         if e is not None:
             land((("rows", f), e[0], e[1]), real(e), piece)
-        elif f == 2:
-            land(("rows x", "second"), None, piece)
         pass_on(("rows", f), e, piece, piece)
-        if f == 0:
-            send(("rows x", e), real(e), piece, piece, partner)
-        if f == 1 and e is None:
-            send(("rows x", "second"), None, piece, piece, partner)
-
-    def rows_cross(e):
-        land(("rows x", e), real(e), lambda: normed.at[span_of(home(e), 3), :])
-
-    def nearest(p):
-        result = 0
-        for zz in range(n):
-            order = sorted(range(n), key=lambda other: (abs(other - zz), other))
-            result = jnp.where(z == zz, order[p], result)
-        return result
-
-    piece_rows = 2 * own_count
-    tile = math.gcd(slab, 256)
-    valid = (first_block(z + 1) - first_block(z)) * BLOCK
-
-    def feed(p):
-        start = pl.multiple_of(nearest(p) * piece_rows, piece_rows)
+
+    half_rows = normed.shape[0] // 2
+    tile = 2 * lanes_down
+
+    def feed(h):
+        span = pl.ds(pl.multiple_of(h * half_rows, half_rows), half_rows)
+
+        def some(cols):
+            x = normed[span, :]
+            gate = jnp.dot(x, wg_all[:, cols], preferred_element_type=jnp.float32)
+            up = jnp.dot(x, wu_all[:, cols], preferred_element_type=jnp.float32)
+            hidden[span, cols] = (gate / (1.0 + jnp.exp(-gate)) * up).astype(jnp.bfloat16)
 
         @pl.loop(0, slab // tile)
         def _(at):
-            cols = pl.ds(pl.multiple_of(at * tile, tile), tile)
-            x = normed[pl.ds(start, piece_rows), :]
-            gate = jnp.dot(x, wg_all[:, cols], preferred_element_type=jnp.float32)
-            up = jnp.dot(x, wu_all[:, cols], preferred_element_type=jnp.float32)
-            unit = at * tile + lax.broadcasted_iota(jnp.int32, gate.shape, 1)
-            product = jnp.where(unit < valid, gate / (1.0 + jnp.exp(-gate)) * up, 0.0)
-            hidden[p * piece_rows:(p + 1) * piece_rows, cols] = product.astype(jnp.bfloat16)
-
-    wide_down = math.gcd(width, 512)
-
-    def lower(p):
-        zz = nearest(p)
-        start = pl.multiple_of(zz * piece_rows, piece_rows)
-
-        @pl.loop(0, width // wide_down)
+            some(pl.ds(pl.multiple_of(at * tile, tile), tile))
+
+        if slab % tile:
+            some(slice(slab - slab % tile, slab))
+
+    groups = 4
+    cols_of = width // groups
+
+    def result_columns(g, at):
+        zs = g % 2 * (n // 2) + at
+        start = (zs * 4 + 2 * (y, other_y)[g // 2]) * lanes_down
+        return pl.ds(pl.multiple_of(start, tile), tile)
+
+    def lower(g):
+        @pl.loop(0, n // 2)
         def _(at):
-            cols = pl.ds(pl.multiple_of(at * wide_down, wide_down), wide_down)
-            part[pl.ds(start, piece_rows), cols] = jnp.dot(
-                hidden[p * piece_rows:(p + 1) * piece_rows, :], wd_all[:, cols],
-                preferred_element_type=jnp.float32,
+            cols = pl.ds(pl.multiple_of(g * cols_of + at * tile, tile), tile)
+            part[:, cols] = jnp.dot(
+                hidden[...], wd_all[:, result_columns(g, at)], preferred_element_type=jnp.float32
             )
 
-        leaving[span_of(zz, 3), :] = part[span_of(zz, 3), :].astype(jnp.bfloat16)
-        send(
-            ("sum x", p), None,
-            lambda: leaving.at[span_of(zz, 3), :], lambda: pair_in.at[zz], partner,
-        )
+    def columns(g):
+        return slice(g * cols_of, (g + 1) * cols_of)
 
     def add(zz, f, ref):
-        part[span_of(zz, f), :] = part[span_of(zz, f), :] + ref[...].astype(jnp.float32)
+        part[whole(zz), columns(f)] = part[whole(zz), columns(f)] + ref[...].astype(jnp.float32)
 
     def sum_send(f, w, d):
         zz = z + d if w == 0 else z - d
@@ -501,12 +544,12 @@
             when(both(inside, room[1 - w]), take)
 
         def put():
-            leaving[span_of(zz, f), :] = part[span_of(zz, f), :].astype(jnp.bfloat16)
+            leaving[whole(zz), columns(f)] = part[whole(zz), columns(f)].astype(jnp.bfloat16)
 
         when(inside, put)
         send(
             ("sum", f, w, d), inside,
-            lambda: leaving.at[span_of(zz, f), :], lambda: line_in.at[f, w, d - 1], ahead[w],
+            lambda: leaving.at[whole(zz), columns(f)], lambda: line_in.at[f, w, d - 1], ahead[w],
         )
 
     def sum_finish(f):
@@ -516,18 +559,25 @@
                 add(z, f, line_in.at[f, w, 0])
 
             when(room[1 - w], take)
-
-    for copy in own:
-        copy.start()
+        for at in range(n // 2):
+            cols = result_columns(f, at)
+            start = f * cols_of + at * tile
+            down = part[whole(z), start:start + tile]
+            out_ref[:, cols] = (mid[:, cols] + 0.5 * down).astype(jnp.bfloat16)
+
+    own_each(lambda copy: copy.start())
+    own_wo.start()
     kv_serve(1, None)
-    send(
-        ("wo", 0), None, lambda: wo_part(wo_in, core), lambda: wo_part(wo_other, core), partner
-    )
-    weight_line(GATE, 1)
     own_rows = pl.ds(pl.multiple_of(sp * tok, tok), tok)
     kv_all[own_rows, :kv_width] = turned_heads(head_size, raw_k, kg_ref, cos_ref, sin_ref)
     kv_all[own_rows, kv_width:] = raw_v[...]
+    for k in range(3):
+        weight_move(k, 0, tp, y, "x")
+        weight_move(k, 0, tp, y, "core")
     kv_serve(0, None)
+    weight_move(GATE, 0, tp, y, "y")
+    for p in range(1, n):
+        weight_line(GATE, p)
     turned = turned_heads(head_size, raw_q, qg_ref, cos_ref, sin_ref).astype(jnp.float32)
     turned = turned * head_size ** (-0.5)
     group = q_rows // (2 * tok)
@@ -543,94 +593,92 @@
             first = (side * group + g + extra) * tok
             q_ref[pair, first:first + tok, :] = kept_lanes.astype(jnp.bfloat16)
 
-    lines = [(k, d) for k in range(3) for d in range(1, n)][1:]
+    def all_lines(k):
+        for p in range(1, n):
+            weight_line(k, p)
+
+    serve = [(k, d) for k in range(3) for d in range(1, n)]
+    over_x = [(k, d) for k in range(3) for d in range(n)]
+    over_y, over_both = list(over_x), list(over_x)
+    queues = {"s": (weight_serve, serve), "x": (cross_x, over_x), "y": (cross_y, over_y), "b": (cross_both, over_both), "l": (all_lines, [(UP,), (DOWN,)])}
+
+    def work(plan):
+        for letter in plan:
+            task, queue = queues[letter]
+            if queue:
+                task(*queue.pop(0))
+
     crossing = [None]
-    for step in arrivals:
+    for at, step in enumerate(arrivals):
         for j in (1, 0):
             for e in step:
                 kv_serve(j, e)
-        weight_line(*lines.pop(0))
+        work(("", "xys", "l")[max(0, at - n + 4)])
         for j in (1, 0):
             for e in crossing:
                 kv_cross(j, e)
         crossing = step
-    for k, d in lines:
-        weight_line(k, d)
-    weight_serve(GATE, 0)
+    work("s")
     for j in (1, 0):
         for e in crossing:
             kv_cross(j, e)
+    work("s")
+    weight_move(UP, 0, tp, y, "y")
     for j in (1, 0):
         for e in events:
             kv_finish(j, e)
-
-    tasks = []
-    served = [(k, d) for k in range(3) for d in range(n)]
-    for at in range(1, len(served)):
-        tasks.append((weight_serve, served[at]))
-        tasks.append((weight_cross, served[at - 1]))
-    tasks.append((weight_cross, served[-1]))
-
-    def work(count):
-        for _ in range(min(count, len(tasks))):
-            task, what = tasks.pop(0)
-            task(*what)
-
+    plans = ["xy", "", "", "xy", "", "l"]
     for at in range(pairs * per_pair):
         attend(at)
-        work(2)
-        if at == 2:
-            land(("wo", 0), None, lambda: wo_part(wo_other, core))
-            send(
-                ("wo", 1), None,
-                lambda: wo_part(wo_other, core), lambda: wo_part(wo_other, core), sibling,
-            )
+        work(plans[at % len(plans)])
     assemble()
-    work(1)
-    send(("context",), None, lambda: context.at[theirs, :], lambda: context_in, partner)
-    work(1)
-    land(("wo", 1), None, lambda: wo_part(wo_other, 1 - core))
-    own[3].wait()
-    land(("context",), None, lambda: context_in)
+    own_wo.wait()
+    project()
+    send(("proj",), None, lambda: proj_out, lambda: proj_in, partner)
+    project_own()
+    weight_move(DOWN, 0, tp, y, "y")
+    work("sxys")
+    land(("proj",), None, lambda: proj_in)
     normalize()
-    work(1)
-    for f in (0, 1):
+    for f in range(2):
         rows_serve(f, None)
-    work(1)
-    rows_serve(2, None)
-    rows_cross(None)
-    work(len(tasks))
-    weight_finish(GATE)
-    weight_finish(UP)
-    feed(0)
-    for at, step in enumerate(arrivals):
-        for f in range(3):
-            for e in step:
+
+    def rows_step(at):
+        for f in range(2):
+            for e in arrivals[at]:
                 rows_serve(f, e)
-        if at == 0:
-            weight_finish(DOWN)
-            lower(0)
-        for e in step:
-            rows_cross(e)
-        feed(at + 1)
-        lower(at + 1)
-    for p in range(n):
-        zz = nearest(p)
-        land(("sum x", p), None, lambda: pair_in.at[zz])
-        add(zz, 0, pair_in.at[zz])
-    for d in range(n - 1, 0, -1):
-        for f in (1, 2, 0):
+
+    work("xysxyxysxyxyss")
+    rows_step(0)
+    while over_both[0][0] < DOWN:
+        work("b")
+    own_each(lambda copy: copy.wait())
+    weight_finish(GATE, (y, other_y))
+    weight_finish(UP, (y, other_y))
+    upper_half = lax.div(z, n // 2)
+    feed(upper_half)
+    for at in range(1, n - 1):
+        work("xy")
+        rows_step(at)
+        work("xy")
+    work("xy" * len(over_x))
+    feed(1 - upper_half)
+    weight_finish(DOWN, (y,))
+    for two in ((0, 1), (2, 3)):
+        if two[0]:
+            work("b" * len(over_both))
+            weight_finish(DOWN, (other_y,))
+        for g in two:
+            lower(g)
             for w in range(2):
-                sum_send(f, w, d)
-    sum_finish(2)
-    leaving[span_of(z, 2), :] = part[span_of(z, 2), :].astype(jnp.bfloat16)
-    sum_finish(0)
-    out_ref[:rows_of, :] = (mid[:rows_of, :] + 0.5 * part[span_of(z, 0), :]).astype(jnp.bfloat16)
-    send(("sum x", "second"), None, lambda: leaving.at[span_of(z, 2), :], lambda: pair_in.at[n], partner)
-    sum_finish(1)
-    land(("sum x", "second"), None, lambda: pair_in.at[n])
-    add(z, 1, pair_in.at[n])
-    out_ref[rows_of:, :] = (mid[rows_of:, :] + 0.5 * part[span_of(z, 1), :]).astype(jnp.bfloat16)
+                sum_send(g, w, n - 1)
+        work("y" * len(over_y))
+        for d in range(n - 2, 0, -1):
+            for g in two:
+                for w in range(2):
+                    sum_send(g, w, d)
+    for g in range(groups):
+        sum_finish(g)
     for condition, make in sent:
         when(condition, lambda: make().wait_send())
     assert len(slots) <= send_sem.shape[0]
@@ -642,6 +690,10 @@
     q_heads = queries.shape[1] // head_size
     kv_heads = keys.shape[1] // head_size
     q_group = q_heads // kv_heads
+    if 2 * w_gate.shape[1] % (n * BLOCK) or n % 2:
+        return body(
+            queries, keys, values, q_gain, k_gain, w_out, residual, norm_gain, w_gate, w_up, w_down
+        )
     n_sp = 4 * n
     positions = lax.axis_index("sp") * tok_rows + jnp.arange(tok_rows, dtype=jnp.int32)
     half_size = head_size // 2
@@ -659,8 +711,8 @@
     own_count, width = residual.shape
     depth_in, units = w_gate.shape
     lanes_down = w_down.shape[1]
-    slab = slab_width(units, n)
-    group_rows = 2 * n * own_count
+    slab = 2 * units // n
+    group_rows = n * own_count
     bf16, f32 = jnp.bfloat16, jnp.float32
     return pl.pallas_call(
         functools.partial(layer_kernel, n, head_size),
@@ -674,17 +726,16 @@
             pltpu.VMEM((n_sp * depth_in, slab), bf16),
             pltpu.VMEM((slab, n_sp * lanes_down), bf16),
             pltpu.VMEM(w_out.shape, bf16),
-            pltpu.VMEM(w_out.shape, bf16),
             pltpu.VMEM(padded, bf16),
             pltpu.VMEM(queries.shape, bf16),
-            pltpu.VMEM((own_count, queries.shape[1]), bf16),
+            pltpu.VMEM((own_count, width), bf16),
+            pltpu.VMEM((own_count, width), bf16),
             pltpu.VMEM((own_count, width), f32),
             pltpu.VMEM((group_rows, width), bf16),
             pltpu.VMEM((group_rows, slab), bf16),
             pltpu.VMEM((group_rows, width), f32),
             pltpu.VMEM((group_rows, width), bf16),
-            pltpu.VMEM((3, 2, n - 1, own_count // 2, width), bf16),
-            pltpu.VMEM((n + 1, own_count // 2, width), bf16),
+            pltpu.VMEM((4, 2, n - 1, own_count, width // 4), bf16),
             pltpu.SemaphoreType.DMA((4,)),
             pltpu.SemaphoreType.DMA((message_count(n),)),
             pltpu.SemaphoreType.DMA((message_count(n),)),

time: 183 us -> 146 us (0.80)
  the two profiles are of different devices: /device:TPU:18 before, /device:TPU:0 now
where the time goes in v2:
time: 146 us
  Pallas kernels  142 us (97%)
  local copies, waits for them, and re-layouts  3.04 us (2%)
    pallas_call x1, Pallas kernels, fast_body(): pl.pallas_call(functools.partial(layer_kernel, n, head_size), out_shape=j...  142 us

profile of v2, /device:TPU:0, one launch (start us, length us, event | category | flops | bytes accessed | tf_op | source)
XLA Modules:
  0.0 145.6 jit_solution(9299515943097200591)
XLA Ops:
  0.0 0.1 broadcast_multiply_fusion
  0.2 0.3 concatenate.3
  0.4 1.0 fusion.3
  1.4 142.4 %layer.1 = bf16[96,2048]{1,0:T(8,128)(2,1)} custom-call(bf16[192,512]{1,0:T(8,128)(2,1)} %raw_q.1, bf16[192,256]{1,0:T(8,128)(2,1)} %raw_k.1, bf16[192,256]{1,0:T(8,128)(2,1)} %raw_v.1, f32[1,64]{1,0:T(1,128)} %bitcast.4, f32[1,64]{1,0:T(1,128)} %bitcast.5, f32[192,128]{1,0:T(8,128)} %get-tuple-element.6.cos_ref, f32[192,128]{1,0:T(8,128)} %get-tuple-element.5.sin_ref, ...), custom_call_target="tpu_custom_call" | custom-call | tf_op jit(solution)/shard_map/layer/pallas_call | solution.py:717
  143.8 1.8 %copy.13 = bf16[96,2048]{1,0:T(8,128)(2,1)} copy(bf16[96,2048]{1,0:T(8,128)(2,1)} %layer.1) | data formatting | bytes 786432
  (2 shorter events, 0.0 us)

commit v3 on v2

--- a/solution.py
+++ b/solution.py
@@ -3,6 +3,7 @@
 
 import jax
 import jax.numpy as jnp
+import numpy as np
 from jax import lax
 from jax.experimental import pallas as pl
 from jax.experimental.pallas import tpu as pltpu
@@ -156,8 +157,9 @@
 
 def message_count(n):
     events = 2 * (n - 1)
-    keys = 2 * events + 6 * (events + 1)
-    return keys + 27 * n + 1 + 2 * events + 8 * n
+    keys_and_values = 2 * events + 2 * (events + 1) + 1
+    weights = 3 * n + 9 * n + 4
+    return keys_and_values + weights + 1 + 2 * events + 8 * (n - 1)
 
 
 def turned_heads(head_size, x_ref, g_ref, cos_ref, sin_ref):
@@ -199,10 +201,10 @@
 
 def layer_kernel(
     n, head_size,
-    raw_q, raw_k, raw_v, qg_ref, kg_ref, cos_ref, sin_ref, res_ref, gain_ref, wo_in, wg_in, wu_in, wd_in,
+    raw_q, raw_k, raw_v, qg_ref, kg_ref, freq_ref, res_ref, gain_ref, wo_in, wg_in, wu_in, wd_in,
     out_ref,
     q_ref, kv_all, wg_all, wu_all, wd_all, wo_own, attn, context, proj_out, proj_in, mid, normed, hidden,
-    part, leaving, line_in, own_sem, send_sem, recv_sem,
+    part, leaving, line_in, out_own, cos_ref, sin_ref, own_sem, out_sem, send_sem, recv_sem,
 ):
     sp = lax.axis_index("sp")
     tp = lax.axis_index("tp")
@@ -237,7 +239,7 @@
         if isinstance(key, tuple):
             slot = slots.setdefault(key, 3 * n + len(slots))
         return pltpu.make_async_remote_copy(
-            src_ref=src, dst_ref=dst, send_sem=send_sem.at[slot], recv_sem=recv_sem.at[slot],
+            src_ref=src, dst_ref=dst, send_sem=send_sem.at[0], recv_sem=recv_sem.at[slot],
             device_id=target, device_id_type=MESH,
         )
 
@@ -296,18 +298,17 @@
         src = (lambda: raw_v) if e is None and j == 1 else dst
         pass_on(("kv", j), e, src, dst)
         send(("kv y", j, e), real(e), src, dst, across)
-        send(("kv core", j, e, 0), real(e), src, dst, sibling)
+        send(("kv core",), real(e), src, dst, sibling)
 
     def kv_cross(j, e):
         def piece():
             return kv_piece(j, home(e), 1 - y, core)
 
         land(("kv y", j, e), real(e), piece)
-        send(("kv core", j, e, 1), real(e), piece, piece, sibling)
-
-    def kv_finish(j, e):
-        land(("kv core", j, e, 0), real(e), lambda: kv_piece(j, home(e), y, 1 - core))
-        land(("kv core", j, e, 1), real(e), lambda: kv_piece(j, home(e), 1 - y, 1 - core))
+        send(("kv core",), real(e), piece, piece, sibling)
+
+    def kv_finish():
+        land(("kv core",), None, lambda: kv_all.at[:kv_all.shape[0] // 2, :])
 
     GATE, UP, DOWN = range(3)
     weights_in = (wg_in, wu_in, wd_in)
@@ -357,7 +358,10 @@
             src = dst
             if p == 0 and corner == (False, False):
                 src = functools.partial(weight_in, k, z, count)
-            send(("w", way, k, p, corner), condition, src, dst, target)
+            key = ("w", way, k, p, corner)
+            if way == "core":
+                key = ("w", way, k, k == DOWN and corner[1])
+            send(key, condition, src, dst, target)
 
     other_x, other_y = 1 - tp, 1 - y
 
@@ -408,12 +412,14 @@
 
     own_wo = pltpu.make_async_copy(wo_in, wo_own, own_sem.at[3])
 
-    def weight_finish(k, sides):
-        for p in range(n):
-            for xx in (tp, other_x):
-                for yy in sides:
-                    corner = (xx is not tp, yy is not y)
-                    weight_take(("w", "core", k, p, corner), k, p, xx, yy, 1 - core)
+    def weight_finish(k, second=False):
+        def bulk():
+            if k == DOWN:
+                return wd_all.at[:, :wd_all.shape[1] // 4]
+            ref = (wg_all, wu_all)[k]
+            return ref.at[:ref.shape[0] // 2, :]
+
+        land(("w", "core", k, second), None, bulk)
 
     pairs, q_rows, lanes = q_ref.shape
     block = math.gcd(q_rows, 256)
@@ -533,9 +539,12 @@
     def add(zz, f, ref):
         part[whole(zz), columns(f)] = part[whole(zz), columns(f)] + ref[...].astype(jnp.float32)
 
-    def sum_send(f, w, d):
+    def sum_step(f, d):
+        for w in range(2):
+            sum_send(f, w, d, z <= n - 1 - d if w == 0 else z >= d)
+
+    def sum_send(f, w, d, inside):
         zz = z + d if w == 0 else z - d
-        inside = z <= n - 1 - d if w == 0 else z >= d
         if d < n - 1:
             def take():
                 message(("sum", f, w, d + 1), line_in.at[f, w, d], line_in.at[f, w, d], partner).wait_recv()
@@ -552,6 +561,12 @@
             lambda: leaving.at[whole(zz), columns(f)], lambda: line_in.at[f, w, d - 1], ahead[w],
         )
 
+    def out_copy(g, at):
+        cols = result_columns(g, at)
+        return pltpu.make_async_copy(
+            out_own.at[:, cols], out_ref.at[:, cols], out_sem.at[g * (n // 2) + at]
+        )
+
     def sum_finish(f):
         for w in range(2):
             def take():
@@ -563,12 +578,20 @@
             cols = result_columns(f, at)
             start = f * cols_of + at * tile
             down = part[whole(z), start:start + tile]
-            out_ref[:, cols] = (mid[:, cols] + 0.5 * down).astype(jnp.bfloat16)
+            out_own[:, cols] = (mid[:, cols] + 0.5 * down).astype(jnp.bfloat16)
+            out_copy(f, at).start()
 
     own_each(lambda copy: copy.start())
     own_wo.start()
     kv_serve(1, None)
     own_rows = pl.ds(pl.multiple_of(sp * tok, tok), tok)
+    at_row = (sp * tok + lax.broadcasted_iota(jnp.int32, cos_ref.shape, 0)).astype(jnp.float32)
+    grid_row = jnp.floor(at_row * (1.0 / GRID_W))
+    lane = lax.broadcasted_iota(jnp.int32, cos_ref.shape, 1)
+    by_row = jnp.bitwise_and(lane, head_size - 1) < head_size // 2
+    angle = jnp.where(by_row, grid_row, at_row - GRID_W * grid_row) * freq_ref[...]
+    cos_ref[...] = jnp.cos(angle)
+    sin_ref[...] = jnp.sin(angle)
     kv_all[own_rows, :kv_width] = turned_heads(head_size, raw_k, kg_ref, cos_ref, sin_ref)
     kv_all[own_rows, kv_width:] = raw_v[...]
     for k in range(3):
@@ -598,8 +621,9 @@
             weight_line(k, p)
 
     serve = [(k, d) for k in range(3) for d in range(1, n)]
-    over_x = [(k, d) for k in range(3) for d in range(n)]
-    over_y, over_both = list(over_x), list(over_x)
+    over_both = [(k, d) for k in range(3) for d in range(n)]
+    over_x = sorted(over_both, key=lambda what: what[1] > 0)
+    over_y = list(over_x)
     queues = {"s": (weight_serve, serve), "x": (cross_x, over_x), "y": (cross_y, over_y), "b": (cross_both, over_both), "l": (all_lines, [(UP,), (DOWN,)])}
 
     def work(plan):
@@ -613,21 +637,23 @@
         for j in (1, 0):
             for e in step:
                 kv_serve(j, e)
+            if at == n - 2:
+                work("s")
+        if at < 2:
+            weight_move(at + 1, 0, tp, y, "y")
         work(("", "xys", "l")[max(0, at - n + 4)])
         for j in (1, 0):
             for e in crossing:
                 kv_cross(j, e)
+        if at == n - 3:
+            work("xy")
         crossing = step
-    work("s")
     for j in (1, 0):
         for e in crossing:
             kv_cross(j, e)
-    work("s")
-    weight_move(UP, 0, tp, y, "y")
-    for j in (1, 0):
-        for e in events:
-            kv_finish(j, e)
-    plans = ["xy", "", "", "xy", "", "l"]
+    work("xy")
+    kv_finish()
+    plans = ["xy", "xy", "xy", "", "", "l"]
     for at in range(pairs * per_pair):
         attend(at)
         work(plans[at % len(plans)])
@@ -636,8 +662,7 @@
     project()
     send(("proj",), None, lambda: proj_out, lambda: proj_in, partner)
     project_own()
-    weight_move(DOWN, 0, tp, y, "y")
-    work("sxys")
+    work("ss")
     land(("proj",), None, lambda: proj_in)
     normalize()
     for f in range(2):
@@ -648,40 +673,50 @@
             for e in arrivals[at]:
                 rows_serve(f, e)
 
-    work("xysxyxysxyxyss")
+    work("xysxy")
     rows_step(0)
+    work("ssxy")
+    while over_both[0][0] < UP:
+        work("b")
+    rows_step(1)
+    work("s")
     while over_both[0][0] < DOWN:
         work("b")
     own_each(lambda copy: copy.wait())
-    weight_finish(GATE, (y, other_y))
-    weight_finish(UP, (y, other_y))
+    weight_finish(GATE)
+    weight_finish(UP)
     upper_half = lax.div(z, n // 2)
     feed(upper_half)
-    for at in range(1, n - 1):
-        work("xy")
+    work("xy")
+    for at in range(2, n - 1):
         rows_step(at)
-        work("xy")
+    work("xy")
+    feed(1 - upper_half)
     work("xy" * len(over_x))
-    feed(1 - upper_half)
-    weight_finish(DOWN, (y,))
+    weight_finish(DOWN)
+    for g in (0, 1):
+        lower(g)
+        sum_step(g, n - 1)
+    for g in (0, 1):
+        sum_step(g, n - 2)
+    work("b" * len(over_both))
+    weight_finish(DOWN, True)
+    for g in (2, 3):
+        lower(g)
+        sum_step(g, n - 1)
     for two in ((0, 1), (2, 3)):
-        if two[0]:
-            work("b" * len(over_both))
-            weight_finish(DOWN, (other_y,))
-        for g in two:
-            lower(g)
-            for w in range(2):
-                sum_send(g, w, n - 1)
-        work("y" * len(over_y))
         for d in range(n - 2, 0, -1):
             for g in two:
-                for w in range(2):
-                    sum_send(g, w, d)
+                if d < n - 2 or g > 1:
+                    sum_step(g, d)
     for g in range(groups):
         sum_finish(g)
+    for g in range(groups):
+        for at in range(n // 2):
+            out_copy(g, at).wait()
     for condition, make in sent:
         when(condition, lambda: make().wait_send())
-    assert len(slots) <= send_sem.shape[0]
+    assert len(slots) + 3 * n == recv_sem.shape[0]
 
 
 def fast_body(n, queries, keys, values, q_gain, k_gain, w_out, residual, norm_gain, w_gate, w_up, w_down):
@@ -695,13 +730,9 @@
             queries, keys, values, q_gain, k_gain, w_out, residual, norm_gain, w_gate, w_up, w_down
         )
     n_sp = 4 * n
-    positions = lax.axis_index("sp") * tok_rows + jnp.arange(tok_rows, dtype=jnp.int32)
     half_size = head_size // 2
-    inv_freq = THETA ** (-jnp.arange(0, half_size, 2, dtype=jnp.float32) / half_size)
-    row_angle = (positions // GRID_W).astype(jnp.float32)[:, None] * inv_freq[None, :]
-    col_angle = (positions % GRID_W).astype(jnp.float32)[:, None] * inv_freq[None, :]
-    angle = jnp.concatenate([row_angle, row_angle, col_angle, col_angle] * 2, axis=1)
-    cos_table, sin_table = jnp.cos(angle), jnp.sin(angle)
+    inv_freq = np.float32(THETA) ** (-np.arange(0, half_size, 2, dtype=np.float32) / half_size)
+    frequencies = jnp.asarray(np.tile(inv_freq, 8)[None, :], jnp.float32)
     pairs = kv_heads // 2
     padded = (pairs, 2 * q_group * tok_rows, 2 * head_size)
     kv_width = keys.shape[1] + values.shape[1]
@@ -717,8 +748,8 @@
     return pl.pallas_call(
         functools.partial(layer_kernel, n, head_size),
         out_shape=jax.ShapeDtypeStruct(residual.shape, bf16),
-        in_specs=[vmem] * 9 + [any_space] * 4,
-        out_specs=vmem,
+        in_specs=[vmem] * 8 + [any_space] * 4,
+        out_specs=any_space,
         scratch_shapes=[
             pltpu.VMEM(padded, bf16),
             pltpu.VMEM((tokens, kv_width), bf16),
@@ -736,8 +767,12 @@
             pltpu.VMEM((group_rows, width), f32),
             pltpu.VMEM((group_rows, width), bf16),
             pltpu.VMEM((4, 2, n - 1, own_count, width // 4), bf16),
+            pltpu.VMEM((own_count, width), bf16),
+            pltpu.VMEM((tok_rows, 2 * head_size), f32),
+            pltpu.VMEM((tok_rows, 2 * head_size), f32),
             pltpu.SemaphoreType.DMA((4,)),
-            pltpu.SemaphoreType.DMA((message_count(n),)),
+            pltpu.SemaphoreType.DMA((2 * n,)),
+            pltpu.SemaphoreType.DMA((1,)),
             pltpu.SemaphoreType.DMA((message_count(n),)),
         ],
         compiler_params=pltpu.CompilerParams(
@@ -745,7 +780,7 @@
         ),
         name="layer",
     )(
-        queries, keys, values, q_gain[None, :], k_gain[None, :], cos_table, sin_table,
+        queries, keys, values, q_gain[None, :], k_gain[None, :], frequencies,
         residual, norm_gain[None, :], w_out, w_gate, w_up, w_down)
 
 

time: 146 us -> 138 us (0.945)
  Pallas kernels: 142 us -> 136 us
    pallas_call x1, Pallas kernels: 142 us -> 136 us  [fast_body(): pl.pallas_call(functools.partial(layer_kernel, n, head_size), out_shape=j...]
where the time goes in v3:
time: 138 us
  Pallas kernels  136 us (99%)
  local copies, waits for them, and re-layouts  1.77 us (1%)
    pallas_call x1, Pallas kernels, fast_body(): pl.pallas_call(functools.partial(layer_kernel, n, head_size), out_shape=j...  136 us

profile of v3, /device:TPU:0, one launch (start us, length us, event | category | flops | bytes accessed | tf_op | source)
XLA Modules:
  0.0 137.6 jit_solution(13283427838035916715)
XLA Ops:
  0.0 135.9 %layer.1 = bf16[96,2048]{1,0:T(8,128)(2,1)} custom-call(bf16[192,512]{1,0:T(8,128)(2,1)} %raw_q.1, bf16[192,256]{1,0:T(8,128)(2,1)} %raw_k.1, bf16[192,256]{1,0:T(8,128)(2,1)} %raw_v.1, f32[1,64]{1,0:T(1,128)} %bitcast.4, f32[1,64]{1,0:T(1,128)} %bitcast.5, f32[1,128]{1,0:T(1,128)} %constant.2.clone.freq_ref, bf16[96,2048]{1,0:T(8,128)(2,1)} %res_ref.1, ...), custom_call_target="tpu_custom_call" | custom-call | tf_op jit(solution)/shard_map/layer/pallas_call | solution.py:748
  135.9 1.8 %copy.14 = bf16[96,2048]{1,0:T(8,128)(2,1)} copy(bf16[96,2048]{1,0:T(8,128)(2,1)} %layer.1) | data formatting | bytes 786432

commit v4 on v3

--- a/solution.py
+++ b/solution.py
@@ -348,7 +348,7 @@
             )
 
     def by_x(k, p):
-        return (p % 4 != 3, p % 2 == 0, p % 2 == 1)[k]
+        return (p % 4 < 2, p % 2 == 0, p % 4 < 2)[k]
 
     def weight_move(k, p, xx, yy, way):
         target = {"x": partner, "y": across, "core": sibling}[way]
@@ -498,17 +498,14 @@
             land((("rows", f), e[0], e[1]), real(e), piece)
         pass_on(("rows", f), e, piece, piece)
 
-    half_rows = normed.shape[0] // 2
     tile = 2 * lanes_down
 
-    def feed(h):
-        span = pl.ds(pl.multiple_of(h * half_rows, half_rows), half_rows)
-
+    def feed():
         def some(cols):
-            x = normed[span, :]
+            x = normed[...]
             gate = jnp.dot(x, wg_all[:, cols], preferred_element_type=jnp.float32)
             up = jnp.dot(x, wu_all[:, cols], preferred_element_type=jnp.float32)
-            hidden[span, cols] = (gate / (1.0 + jnp.exp(-gate)) * up).astype(jnp.bfloat16)
+            hidden[:, cols] = (gate / (1.0 + jnp.exp(-gate)) * up).astype(jnp.bfloat16)
 
         @pl.loop(0, slab // tile)
         def _(at):
@@ -539,9 +536,12 @@
     def add(zz, f, ref):
         part[whole(zz), columns(f)] = part[whole(zz), columns(f)] + ref[...].astype(jnp.float32)
 
-    def sum_step(f, d):
+    def sum_step(f, d, ends=None):
         for w in range(2):
-            sum_send(f, w, d, z <= n - 1 - d if w == 0 else z >= d)
+            inside = z <= n - 1 - d if w == 0 else z >= d
+            if ends is not None:
+                inside = both(inside, jnp.logical_not(room[1 - w]) if ends else room[1 - w])
+            sum_send(f, w, d, inside)
 
     def sum_send(f, w, d, inside):
         zz = z + d if w == 0 else z - d
@@ -637,11 +637,9 @@
         for j in (1, 0):
             for e in step:
                 kv_serve(j, e)
-            if at == n - 2:
-                work("s")
-        if at < 2:
-            weight_move(at + 1, 0, tp, y, "y")
-        work(("", "xys", "l")[max(0, at - n + 4)])
+        if at == 0:
+            weight_move(UP, 0, tp, y, "y")
+        work(("", "xys", "ssl")[max(0, at - n + 4)])
         for j in (1, 0):
             for e in crossing:
                 kv_cross(j, e)
@@ -651,9 +649,9 @@
     for j in (1, 0):
         for e in crossing:
             kv_cross(j, e)
-    work("xy")
+    weight_move(DOWN, 0, tp, y, "y")
     kv_finish()
-    plans = ["xy", "xy", "xy", "", "", "l"]
+    plans = ["", "", "", "", "", "l"]
     for at in range(pairs * per_pair):
         attend(at)
         work(plans[at % len(plans)])
@@ -662,7 +660,7 @@
     project()
     send(("proj",), None, lambda: proj_out, lambda: proj_in, partner)
     project_own()
-    work("ss")
+    work("xyxyxysxys")
     land(("proj",), None, lambda: proj_in)
     normalize()
     for f in range(2):
@@ -675,7 +673,7 @@
 
     work("xysxy")
     rows_step(0)
-    work("ssxy")
+    work("xyss")
     while over_both[0][0] < UP:
         work("b")
     rows_step(1)
@@ -685,13 +683,10 @@
     own_each(lambda copy: copy.wait())
     weight_finish(GATE)
     weight_finish(UP)
-    upper_half = lax.div(z, n // 2)
-    feed(upper_half)
-    work("xy")
     for at in range(2, n - 1):
         rows_step(at)
     work("xy")
-    feed(1 - upper_half)
+    feed()
     work("xy" * len(over_x))
     weight_finish(DOWN)
     for g in (0, 1):
@@ -708,7 +703,9 @@
         for d in range(n - 2, 0, -1):
             for g in two:
                 if d < n - 2 or g > 1:
-                    sum_step(g, d)
+                    sum_step(g, d, False if d == 1 else None)
+    for g in range(groups):
+        sum_step(g, 1, True)
     for g in range(groups):
         sum_finish(g)
     for g in range(groups):

time: 138 us -> 133 us (0.964)
  Pallas kernels: 136 us -> 131 us
    pallas_call x1, Pallas kernels: 136 us -> 131 us  [fast_body(): pl.pallas_call(functools.partial(layer_kernel, n, head_size), out_shape=j...]
where the time goes in v4:
time: 133 us
  Pallas kernels  131 us (98%)
  local copies, waits for them, and re-layouts  1.77 us (1%)
    pallas_call x1, Pallas kernels, fast_body(): pl.pallas_call(functools.partial(layer_kernel, n, head_size), out_shape=j...  131 us

profile of v4, /device:TPU:0, one launch (start us, length us, event | category | flops | bytes accessed | tf_op | source)
XLA Modules:
  0.0 133.2 jit_solution(5428836314184840338)
XLA Ops:
  0.0 131.4 %layer.1 = bf16[96,2048]{1,0:T(8,128)(2,1)} custom-call(bf16[192,512]{1,0:T(8,128)(2,1)} %raw_q.1, bf16[192,256]{1,0:T(8,128)(2,1)} %raw_k.1, bf16[192,256]{1,0:T(8,128)(2,1)} %raw_v.1, f32[1,64]{1,0:T(1,128)} %bitcast.4, f32[1,64]{1,0:T(1,128)} %bitcast.5, f32[1,128]{1,0:T(1,128)} %constant.2.clone.freq_ref, bf16[96,2048]{1,0:T(8,128)(2,1)} %res_ref.1, ...), custom_call_target="tpu_custom_call" | custom-call | tf_op jit(solution)/shard_map/layer/pallas_call | solution.py:745
  131.4 1.8 %copy.14 = bf16[96,2048]{1,0:T(8,128)(2,1)} copy(bf16[96,2048]{1,0:T(8,128)(2,1)} %layer.1) | data formatting | bytes 786432

commit v5 on v4

--- a/solution.py
+++ b/solution.py
@@ -617,7 +617,7 @@
             q_ref[pair, first:first + tok, :] = kept_lanes.astype(jnp.bfloat16)
 
     def all_lines(k):
-        for p in range(1, n):
+        for p in range(2 if k == UP else 1, n):
             weight_line(k, p)
 
     serve = [(k, d) for k in range(3) for d in range(1, n)]
@@ -640,6 +640,8 @@
         if at == 0:
             weight_move(UP, 0, tp, y, "y")
         work(("", "xys", "ssl")[max(0, at - n + 4)])
+        if at == n - 3:
+            weight_line(UP, 1)
         for j in (1, 0):
             for e in crossing:
                 kv_cross(j, e)
@@ -651,7 +653,7 @@
             kv_cross(j, e)
     weight_move(DOWN, 0, tp, y, "y")
     kv_finish()
-    plans = ["", "", "", "", "", "l"]
+    plans = ["", "", "", "s", "", "l"]
     for at in range(pairs * per_pair):
         attend(at)
         work(plans[at % len(plans)])
@@ -660,7 +662,7 @@
     project()
     send(("proj",), None, lambda: proj_out, lambda: proj_in, partner)
     project_own()
-    work("xyxyxysxys")
+    work("xyxyxyxys")
     land(("proj",), None, lambda: proj_in)
     normalize()
     for f in range(2):

time: 133 us -> 133 us (level)
  no operation moved by 1% of the time
where the time goes in v5:
time: 133 us
  Pallas kernels  131 us (98%)
  local copies, waits for them, and re-layouts  1.77 us (1%)
    pallas_call x1, Pallas kernels, fast_body(): pl.pallas_call(functools.partial(layer_kernel, n, head_size), out_shape=j...  131 us

profile of v5, /device:TPU:0, one launch (start us, length us, event | category | flops | bytes accessed | tf_op | source)
XLA Modules:
  0.0 133.2 jit_solution(8386307575472512533)
XLA Ops:
  0.0 131.4 %layer.1 = bf16[96,2048]{1,0:T(8,128)(2,1)} custom-call(bf16[192,512]{1,0:T(8,128)(2,1)} %raw_q.1, bf16[192,256]{1,0:T(8,128)(2,1)} %raw_k.1, bf16[192,256]{1,0:T(8,128)(2,1)} %raw_v.1, f32[1,64]{1,0:T(1,128)} %bitcast.4, f32[1,64]{1,0:T(1,128)} %bitcast.5, f32[1,128]{1,0:T(1,128)} %constant.2.clone.freq_ref, bf16[96,2048]{1,0:T(8,128)(2,1)} %res_ref.1, ...), custom_call_target="tpu_custom_call" | custom-call | tf_op jit(solution)/shard_map/layer/pallas_call | solution.py:747
  131.4 1.8 %copy.14 = bf16[96,2048]{1,0:T(8,128)(2,1)} copy(bf16[96,2048]{1,0:T(8,128)(2,1)} %layer.1) | data formatting | bytes 786432
